TPU v7x, 32 devices: a whole 2x2x4 slice. The times are simulated.
32 devices in a mesh: sp: 8 (over z, x), tp: 4 (over y, core).
Axes of the slice: x: 2, y: 2, z: 4, core: 2. Of those that a mesh axis runs over, the one named last changes fastest.
Arguments:
- stream_in: bfloat16 [1024, 2048], P('sp'), may hold values from -8 to 8
- out_cot: bfloat16 [1024, 2048], P('sp'), may hold values from -6 to 6
- route_experts: int32 [1024, 2], P('sp'), may hold values from 0 to 7, all different within a row; in each aligned block of 128 rows (0 to 127, 128 to 255, ...) at most 64 rows name the same one
- route_weights: float32 [1024, 2], P('sp'), may hold values from 0.1 to 1
- w_gate: bfloat16 [8, 2048, 2048], P('sp', None, 'tp'), may hold values from -0.125 to 0.125
- w_up: bfloat16 [8, 2048, 2048], P('sp', None, 'tp'), may hold values from -0.125 to 0.125
- w_down: bfloat16 [8, 2048, 2048], P('sp', 'tp'), may hold values from -0.125 to 0.125
- w_proj: bfloat16 [2048, 1024], P(None, 'tp'), may hold values from -0.1875 to 0.1875
- conv_value: bfloat16 [1024, 1024], P('tp', 'sp'), may hold values from -6 to 6
- conv_gate: bfloat16 [1024, 1024], P('tp', 'sp'), may hold values from -8 to 8
- conv_taps: float32 [31, 1024], P(None, 'tp'), may hold values from -1 to 1
- conv_result: bfloat16 [1024, 1024], P('tp', 'sp'), may hold values from -100 to 100
- channel_norm_gain: float32 [1024], P('tp'), may hold values from 0.1 to 1.9
Outputs:
- grad_gate: bfloat16 [8, 2048, 2048], P('sp', None, 'tp')
- grad_up: bfloat16 [8, 2048, 2048], P('sp', None, 'tp')
- grad_down: bfloat16 [8, 2048, 2048], P('sp', 'tp')
- grad_stream: bfloat16 [1024, 2048], P('sp')
- grad_proj: float32 [2048, 1024], P('sp', 'tp')
- grad_value: bfloat16 [1024, 1024], P('tp', 'sp')
- grad_gate_in: bfloat16 [1024, 1024], P('tp', 'sp')
Inputs may be any that keep to these rules, and one draw needn't show every extreme that they name: `route_experts`: each row names 2 different experts; within each aligned block of 128 rows no expert is named by more than 64 rows, and at least one block reaches that bound for some expert.
All inputs are finite; a program needn't handle non-finite values.
Results may differ from a plain program's by a relative error of at most 0.025.
Values may be sent and summed in bfloat16 or wider, within the bound.
A program may use at most 64 MiB of HBM per device.

v0:
```python
import functools

import jax
import jax.numpy as jnp
from jax import lax
from jax.experimental import pallas as pl
from jax.experimental.pallas import tpu as pltpu
from jax.sharding import PartitionSpec as P

norm_eps = 1e-05
clamp_limit = 7.0
alpha_gate = 1.702
MESH = pl.DeviceIdType.MESH
f32 = jnp.float32
bf16 = jnp.bfloat16


def dot(a, b, ca=1, cb=0):
    return lax.dot_general(a, b, (((ca,), (cb,)), ((), ())), preferred_element_type=f32)


def aligned(start, size):
    return pl.ds(pl.multiple_of(start, size), size)


def greet(n, s, q, tp_peers):
    barrier = pltpu.get_barrier_semaphore()
    for d in range(1, n):
        pl.semaphore_signal(
            barrier, inc=1, device_id={"sp": lax.rem(s + d, n), "tp": q}, device_id_type=MESH
        )
    for peer in tp_peers:
        pl.semaphore_signal(barrier, inc=1, device_id={"sp": s, "tp": peer}, device_id_type=MESH)
    pl.semaphore_wait(barrier, n - 1 + len(tp_peers))


def remote(src, dst, send, recv, sp, tp):
    return pltpu.make_async_remote_copy(
        src_ref=src,
        dst_ref=dst,
        send_sem=send,
        recv_sem=recv,
        device_id={"sp": sp, "tp": tp},
        device_id_type=MESH,
    )


def partners(q):
    core, other = lax.rem(q, 2), q // 2
    return (2 * other + 1 - core, 2 * (1 - other) + core, 2 * (1 - other) + 1 - core)


def dispatch_kernel(
    n, cap, routes_ref, weights_ref, stream_ref, cot_ref, rows_ref, cots_ref, pick_ref,
    weighted_ref, stage, send_xz, recv_xz, send_y, recv_y, send_c, recv_c, send_d, recv_d,
):
    s, q = lax.axis_index("sp"), lax.axis_index("tp")
    q_core, q_y, q_far = partners(q)
    top, tokens = routes_ref.shape
    width = stage.shape[-1]
    slots = pick_ref.shape[0]
    experts = slots // cap

    greet(n, s, q, (q_core, q_y))

    routes = routes_ref[...]
    expert_ids = lax.broadcasted_iota(jnp.int32, (experts, tokens), 0)
    hits = [expert_ids == routes[k : k + 1, :] for k in range(top)]
    count = sum(h.astype(f32) for h in hits)
    earlier = (
        lax.broadcasted_iota(jnp.int32, (tokens, tokens), 0)
        < lax.broadcasted_iota(jnp.int32, (tokens, tokens), 1)
    ).astype(f32)
    before = dot(count.astype(bf16), earlier.astype(bf16))
    slot_ids = lax.broadcasted_iota(jnp.int32, (slots, tokens), 0)
    pick = jnp.zeros((slots, tokens), f32)
    weighted = jnp.zeros((slots, tokens), f32)
    for k in range(top):
        rank = jnp.sum(jnp.where(hits[k], before, 0.0), axis=0, keepdims=True)
        slot = routes[k : k + 1, :] * cap + rank.astype(jnp.int32)
        here = slot_ids == slot
        pick = jnp.where(here, 1.0, pick)
        weighted = jnp.where(here, weights_ref[k : k + 1, :], weighted)
    slot_weight = jnp.sum(weighted, axis=1, keepdims=True)
    pick = pick.astype(bf16)
    pick_ref[...] = pick
    weighted_ref[...] = weighted
    own = aligned(q * width, width)
    picked = dot(pick, stream_ref[:, own]).astype(bf16)
    stage[0] = picked
    stage[1] = (slot_weight * dot(pick, cot_ref[:, own])).astype(bf16)

    outs = (rows_ref, cots_ref)
    copies = []

    def start(copy):
        copy.start()
        copies.append(copy)
        return copy

    def at(a, source, quarter):
        return outs[a].at[aligned(source * cap, cap), aligned(quarter * width, width)]

    arriving = []
    for d in range(1, n):
        dest = lax.rem(s + d, n)
        arriving.append(
            [
                start(
                    remote(
                        stage.at[a, aligned(dest * cap, cap)], at(a, s, q),
                        send_xz.at[a, d], recv_xz.at[a, d], dest, q,
                    )
                )
                for a in range(2)
            ]
        )
    mine = aligned(s * cap, cap)
    rows_ref[mine, :] = dot(pick_ref[mine, :], stream_ref[...]).astype(bf16)
    cots_ref[mine, :] = (
        jnp.sum(weighted_ref[mine, :], axis=1, keepdims=True)
        * dot(pick_ref[mine, :], cot_ref[...])
    ).astype(bf16)

    across, tail = [None], []

    def far_forward(d):
        source = lax.rem(s + n - d, n)
        for a in range(2):
            across[d][a].wait_recv()
            tail.append(
                start(
                    remote(
                        at(a, source, q_y), at(a, source, q_y),
                        send_d.at[a, d], recv_d.at[a, d], s, q_core,
                    )
                )
            )

    for d in range(1, n):
        source = lax.rem(s + n - d, n)
        row = []
        for a in range(2):
            arriving[d - 1][a].wait_recv()
            block = at(a, source, q)
            row.append(start(remote(block, block, send_y.at[a, d], recv_y.at[a, d], s, q_y)))
            tail.append(start(remote(block, block, send_c.at[a, d], recv_c.at[a, d], s, q_core)))
        across.append(row)
        if d > 1:
            far_forward(d - 1)
    far_forward(n - 1)
    for copy in tail:
        copy.wait_recv()
    for copy in copies:
        copy.wait_send()


def dispatch(stream_in, out_cot, routes, weights, n, cap, tp_count, experts):
    tokens, model_width = stream_in.shape
    width = model_width // tp_count
    slots = experts * cap
    dma = [pltpu.SemaphoreType.DMA((2, n))] * 8
    return pl.pallas_call(
        functools.partial(dispatch_kernel, n, cap),
        out_shape=(
            jax.ShapeDtypeStruct((n * cap, model_width), bf16),
            jax.ShapeDtypeStruct((n * cap, model_width), bf16),
            jax.ShapeDtypeStruct((slots, tokens), bf16),
        ),
        in_specs=[pl.BlockSpec(memory_space=pltpu.VMEM)] * 4,
        out_specs=[pl.BlockSpec(memory_space=pltpu.VMEM)] * 3,
        scratch_shapes=[
            pltpu.VMEM((slots, tokens), f32),
            pltpu.VMEM((2, slots, width), bf16),
        ]
        + dma,
        compiler_params=pltpu.CompilerParams(
            collective_id=0, has_side_effects=True, vmem_limit_bytes=24 << 20
        ),
        name="dispatch",
    )(routes, weights, stream_in, out_cot)


def tail_kernel(
    n, cap, channel_total,
    part_ref, pick_ref, cot_ref, proj_ref, value_ref, gate_ref, taps_ref, conv_ref, gain_ref,
    gs_ref, gproj_ref, gvalue_ref, ggate_ref,
    from_core, own, to_y, from_y, to_xz, ret, hid_all, col_all, stat, stat2, ext,
    send_c, recv_c, send_y, recv_y, send_r, recv_r, send_h, recv_h, send_s, recv_s,
    send_g, recv_g, send_k, recv_k, send_f, recv_f, send_e, recv_e,
):
    s, q = lax.axis_index("sp"), lax.axis_index("tp")
    q_core, q_y, q_far = partners(q)
    peers = (q_core, q_y, q_far)
    core, y = lax.rem(q, 2), q // 2
    tokens, model_width = gs_ref.shape
    width = ret.shape[-1]
    icols = gproj_ref.shape[0]
    taps_count = taps_ref.shape[0]
    copies = []

    def start(copy):
        copy.start()
        copies.append(copy)
        return copy

    greet(n, s, q, peers)

    order = [lax.rem(s + d, n) for d in range(1, n)] + [s]
    from_c = []
    for j, b in enumerate(order):
        rows = aligned(b * cap, cap)
        from_c.append(
            [
                start(
                    remote(
                        part_ref.at[rows, aligned((2 * half + 1 - core) * width, width)],
                        from_core.at[h, rows],
                        send_c.at[h, j], recv_c.at[h, j], s, q_core,
                    )
                )
                for h, half in ((0, 1 - y), (1, y))
            ]
        )

    def exchange_stats(buffer, first, second, which):
        lanes = lax.broadcasted_iota(jnp.int32, (tokens, tokens), 1)
        packed = jnp.where(lanes == 0, first, jnp.where(lanes == 1, second, 0.0))
        buffer[3] = packed.T[0:8, :]
        return [
            start(
                remote(
                    buffer.at[3], buffer.at[p], send_s.at[which, p], recv_s.at[which, p], s, peer
                )
            )
            for p, peer in enumerate(peers)
        ]

    def summed_stats(buffer, waits):
        for w in waits:
            w.wait_recv()
        total = (buffer[3] + buffer[0]) + (buffer[1] + buffer[2])
        wide = jnp.concatenate([total, jnp.zeros((tokens - 8, tokens), f32)], axis=0).T
        return wide[:, 0:1], wide[:, 1:2]

    conv = conv_ref[...].astype(f32).T
    stat_waits = exchange_stats(
        stat,
        jnp.sum(conv, axis=1, keepdims=True),
        jnp.sum(conv * conv, axis=1, keepdims=True),
        0,
    )
    over_y = []
    for j, b in enumerate(order):
        rows = aligned(b * cap, cap)
        from_c[j][0].wait_recv()
        to_y[rows, :] = (
            part_ref[rows, aligned((2 * (1 - y) + core) * width, width)].astype(f32)
            + from_core[0, rows, :].astype(f32)
        ).astype(bf16)
        over_y.append(
            start(
                remote(to_y.at[rows], from_y.at[rows], send_y.at[j], recv_y.at[j], s, q_y)
            )
        )
    for j, b in enumerate(order):
        rows = aligned(b * cap, cap)
        from_c[j][1].wait_recv()
        own[rows, :] = part_ref[rows, aligned(q * width, width)].astype(f32) + from_core[
            1, rows, :
        ].astype(f32)
    chan_sum, chan_sq = summed_stats(stat, stat_waits)
    chan_mean = chan_sum / channel_total
    chan_var = chan_sq / channel_total - chan_mean * chan_mean
    inverse_deviation = lax.rsqrt(chan_var + norm_eps)
    mean_removed = (conv - chan_mean) * inverse_deviation
    gain = gain_ref[...]
    normed = mean_removed * gain
    sig = jax.nn.sigmoid(normed)
    hid_all[aligned(s * tokens, tokens), :] = (normed * sig).astype(bf16)
    slope = sig * (1.0 + normed * (1.0 - sig)) * gain
    back = []
    for j, b in enumerate(order):
        rows = aligned(b * cap, cap)
        over_y[j].wait_recv()
        total = (own[rows, :] + from_y[rows, :].astype(f32)).astype(bf16)
        if j == n - 1:
            ret[rows, :] = total
        else:
            to_xz[rows, :] = total
            back.append(
                start(
                    remote(
                        to_xz.at[rows], ret.at[aligned(s * cap, cap)],
                        send_r.at[j], recv_r.at[j], b, q,
                    )
                )
            )
    mine = aligned(s * tokens, tokens)
    hid_waits = [
        start(
            remote(hid_all.at[mine], hid_all.at[mine], send_h.at[j], recv_h.at[j], order[j], q)
        )
        for j in range(n - 1)
    ]
    for copy in back:
        copy.wait_recv()
    quarter = aligned(q * width, width)
    combined = dot(pick_ref[...], ret[...], 0, 0) + cot_ref[:, quarter].astype(f32)
    gs_ref[:, quarter] = combined.astype(bf16)
    quarter_y = aligned(q_y * width, width)
    by_core = start(
        remote(gs_ref.at[:, quarter], gs_ref.at[:, quarter], send_g.at[0], recv_g.at[0], s, q_core)
    )
    by_y = start(
        remote(gs_ref.at[:, quarter], gs_ref.at[:, quarter], send_g.at[1], recv_g.at[1], s, q_y)
    )

    def partial_of(owner):
        cols = aligned(owner * width, width)
        return dot(gs_ref[:, cols], proj_ref[cols, :])

    grad_hidden = partial_of(q)
    by_y.wait_recv()
    by_far = start(
        remote(
            gs_ref.at[:, quarter_y], gs_ref.at[:, quarter_y], send_g.at[2], recv_g.at[2], s, q_core
        )
    )
    grad_hidden = grad_hidden + partial_of(q_y)
    by_core.wait_recv()
    grad_hidden = grad_hidden + partial_of(q_core)
    by_far.wait_recv()
    grad_hidden = grad_hidden + partial_of(q_far)
    half_rows = tokens // 2
    part_rows = aligned(core * half_rows, half_rows)
    land = aligned(s * tokens + core * half_rows, half_rows)
    col_waits = [
        start(
            remote(
                gs_ref.at[part_rows, aligned(order[j] * icols, icols)], col_all.at[land],
                send_k.at[j], recv_k.at[j], order[j], q,
            )
        )
        for j in range(n - 1)
    ]
    col_all[mine, :] = gs_ref[:, aligned(s * icols, icols)]
    norm_grad = grad_hidden * slope
    stat_waits = exchange_stats(
        stat2,
        jnp.sum(norm_grad, axis=1, keepdims=True),
        jnp.sum(norm_grad * mean_removed, axis=1, keepdims=True),
        1,
    )
    avg, cross = summed_stats(stat2, stat_waits)
    conv_grad = inverse_deviation * (
        norm_grad - avg / channel_total - mean_removed * (cross / channel_total)
    )
    rim = ext.shape[0] - tokens
    ext[0:tokens, :] = conv_grad
    halo = start(
        remote(
            ext.at[0:rim], ext.at[tokens : tokens + rim], send_e.at[0], recv_e.at[0],
            lax.rem(s + n - 1, n), q,
        )
    )
    forwards = []
    for j in range(n - 1):
        col_waits[j].wait_recv()
        source = lax.rem(s + n - (j + 1), n)
        there = aligned(source * tokens + core * half_rows, half_rows)
        forwards.append(
            start(
                remote(col_all.at[there], col_all.at[there], send_f.at[j], recv_f.at[j], s, q_core)
            )
        )
    halo.wait_recv()
    edge = ext[tokens : tokens + rim, :]
    halo.wait_send()
    ext[tokens : tokens + rim, :] = jnp.where(s == n - 1, 0.0, edge)
    acc = jnp.zeros((tokens, ext.shape[1]), f32)
    for tap in range(taps_count):
        acc = acc + taps_ref[tap : tap + 1, :] * ext[tap : tap + tokens, :]
    gated = acc.T
    gate_sig = jax.nn.sigmoid(gate_ref[...].astype(f32))
    gvalue_ref[...] = (gated * gate_sig).astype(bf16)
    ggate_ref[...] = (
        gated * value_ref[...].astype(f32) * gate_sig * (1.0 - gate_sig)
    ).astype(bf16)
    for copy in hid_waits + forwards:
        copy.wait_recv()
    gproj_ref[...] = dot(col_all[...], hid_all[...], 0, 0)
    for copy in copies:
        if copy is not halo:
            copy.wait_send()


def tail(part, pick, out_cot, w_proj, value, gate, taps, conv, gain, n, cap, tp_count):
    tokens, model_width = out_cot.shape
    width = model_width // tp_count
    channels = value.shape[0]
    icols = model_width // n
    slots = pick.shape[0]
    rows = part.shape[0]
    rim = -(-(taps.shape[0] - 1) // 8) * 8
    V = pltpu.VMEM
    dma = pltpu.SemaphoreType.DMA
    pairs = [(2, n), (n,), (n,), (n,), (2, 3), (3,), (n,), (n,), (1,)]
    return pl.pallas_call(
        functools.partial(tail_kernel, n, cap, channels * tp_count),
        out_shape=(
            jax.ShapeDtypeStruct((tokens, model_width), bf16),
            jax.ShapeDtypeStruct((icols, channels), f32),
            jax.ShapeDtypeStruct((channels, tokens), bf16),
            jax.ShapeDtypeStruct((channels, tokens), bf16),
        ),
        in_specs=[pl.BlockSpec(memory_space=V)] * 9,
        out_specs=[pl.BlockSpec(memory_space=V)] * 4,
        scratch_shapes=[
            V((2, rows, width), bf16),
            V((rows, width), f32),
            V((rows, width), bf16),
            V((rows, width), bf16),
            V((rows, width), bf16),
            V((slots, width), bf16),
            V((n * tokens, channels), bf16),
            V((n * tokens, icols), bf16),
            V((4, 8, tokens), f32),
            V((4, 8, tokens), f32),
            V((tokens + rim, channels), f32),
        ]
        + [dma(shape) for shape in pairs for _ in range(2)],
        compiler_params=pltpu.CompilerParams(
            collective_id=1, has_side_effects=True, vmem_limit_bytes=40 << 20
        ),
        name="combine_tail",
    )(part, pick, out_cot, w_proj, value, gate, taps, conv, gain)


def flush_kernel(*refs):
    count = len(refs) // 2
    copies = [
        pltpu.make_async_copy(refs[i], refs[count + i], refs[-1].at[i]) for i in range(count)
    ]
    for copy in copies:
        copy.start()
    for copy in copies:
        copy.wait()


def flush(*arrays):
    return pl.pallas_call(
        flush_kernel,
        out_shape=tuple(jax.ShapeDtypeStruct(a.shape, a.dtype) for a in arrays),
        in_specs=[pl.BlockSpec(memory_space=pltpu.VMEM)] * len(arrays),
        out_specs=[pl.BlockSpec(memory_space=pltpu.HBM)] * len(arrays),
        scratch_shapes=[pltpu.SemaphoreType.DMA((len(arrays),))],
        compiler_params=pltpu.CompilerParams(vmem_limit_bytes=4 << 20),
        name="flush",
    )(*arrays)


def expert_terms(rows_in, cot_in, w_gate, w_up, w_down):
    pre_gate = dot(rows_in, w_gate)
    pre_up = dot(rows_in, w_up)
    glu_part = jnp.minimum(pre_gate, clamp_limit)
    lin_part = jnp.clip(pre_up, -clamp_limit, clamp_limit)
    sig_glu = jax.nn.sigmoid(alpha_gate * glu_part)
    activated = (glu_part * sig_glu * (lin_part + 1.0)).astype(bf16)
    grad_act = dot(cot_in, w_down, 1, 1)
    slope = sig_glu + alpha_gate * glu_part * sig_glu * (1.0 - sig_glu)
    grad_pre_gate = jnp.where(
        pre_gate < clamp_limit, grad_act * (lin_part + 1.0) * slope, 0.0
    ).astype(bf16)
    grad_pre_up = jnp.where(
        jnp.abs(pre_up) < clamp_limit, grad_act * glu_part * sig_glu, 0.0
    ).astype(bf16)
    grad_down = dot(activated, cot_in, 0, 0).astype(bf16)
    grad_gate = dot(rows_in, grad_pre_gate, 0, 0).astype(bf16)
    grad_up = dot(rows_in, grad_pre_up, 0, 0).astype(bf16)
    input_part = dot(grad_pre_gate, w_gate, 1, 1) + dot(grad_pre_up, w_up, 1, 1)
    return (grad_gate, grad_up, grad_down, input_part.astype(bf16))


def body(
    stream_in, out_cot, route_experts, route_weights, w_gate, w_up, w_down, w_proj,
    conv_value, conv_gate, conv_taps, conv_result, channel_norm_gain,
):
    n = lax.axis_size("sp")
    tp_count = lax.axis_size("tp")
    experts = w_gate.shape[0] * n
    tokens, model_width = stream_in.shape
    cap = 2 * route_experts.shape[1] * tokens // experts
    rows_in, cot_in, pick = dispatch(
        stream_in, out_cot, route_experts.T, route_weights.T, n, cap, tp_count, experts
    )
    grad_gate, grad_up, grad_down, part = expert_terms(
        rows_in, cot_in, w_gate[0], w_up[0], w_down[0]
    )
    grad_stream, grad_proj, grad_value, grad_gate_in = tail(
        part, pick, out_cot, w_proj, conv_value, conv_gate, conv_taps, conv_result,
        channel_norm_gain[None, :], n, cap, tp_count,
    )
    grad_stream, grad_proj, grad_value, grad_gate_in = flush(
        grad_stream, grad_proj, grad_value, grad_gate_in
    )
    return (
        grad_gate[None], grad_up[None], grad_down[None],
        grad_stream, grad_proj, grad_value, grad_gate_in,
    )


def from_behind(value, axis, steps):
    count = lax.axis_size(axis)
    leading, last = (max(0, -steps), min(count, count - steps))
    return lax.ppermute(value, axis, [(source, source + steps) for source in range(leading, last)])


def slot_tables(block_routes, experts_all, capacity):
    flat_routes = block_routes.reshape(-1)
    assigns = flat_routes.shape[0]
    onehot = (flat_routes[:, None] == jnp.arange(experts_all, dtype=jnp.int32)[None, :]).astype(
        jnp.int32
    )
    before = jnp.cumsum(onehot, axis=0) - onehot
    rank_in = jnp.sum(before * onehot, axis=1)
    slot_of = flat_routes * capacity + rank_in
    source_of = (
        jnp.full((experts_all * capacity,), -1, jnp.int32)
        .at[slot_of]
        .set(jnp.arange(assigns, dtype=jnp.int32))
    )
    return (slot_of, source_of)


def combine_routes(returned, slot_of, cot_cols, token_rows, top_count):
    feature_count = returned.shape[-1]
    flat_back = returned.reshape(-1, feature_count)
    per_route = flat_back[slot_of].astype(jnp.float32).reshape(token_rows, top_count, feature_count)
    return (cot_cols.astype(jnp.float32) + jnp.sum(per_route, axis=1)).astype(jnp.bfloat16)


def expert_terms_plain(rows_in, cot_in, w_gate, w_up, w_down):
    pre_gate = jnp.einsum("secd,edf->secf", rows_in, w_gate, preferred_element_type=jnp.float32)
    pre_up = jnp.einsum("secd,edf->secf", rows_in, w_up, preferred_element_type=jnp.float32)
    glu_part = jnp.minimum(pre_gate, clamp_limit)
    lin_part = jnp.clip(pre_up, -clamp_limit, clamp_limit)
    sig_glu = jax.nn.sigmoid(alpha_gate * glu_part)
    activated = (glu_part * sig_glu * (lin_part + 1.0)).astype(jnp.bfloat16)
    grad_act = jnp.einsum("secd,efd->secf", cot_in, w_down, preferred_element_type=jnp.float32)
    slope = sig_glu + alpha_gate * glu_part * sig_glu * (1.0 - sig_glu)
    grad_pre_gate = jnp.where(
        pre_gate < clamp_limit, grad_act * (lin_part + 1.0) * slope, 0.0
    ).astype(jnp.bfloat16)
    grad_pre_up = jnp.where(
        jnp.abs(pre_up) < clamp_limit, grad_act * glu_part * sig_glu, 0.0
    ).astype(jnp.bfloat16)
    grad_down = jnp.einsum(
        "secf,secd->efd", activated, cot_in, preferred_element_type=jnp.float32
    ).astype(jnp.bfloat16)
    grad_gate = jnp.einsum(
        "secd,secf->edf", rows_in, grad_pre_gate, preferred_element_type=jnp.float32
    ).astype(jnp.bfloat16)
    grad_up = jnp.einsum(
        "secd,secf->edf", rows_in, grad_pre_up, preferred_element_type=jnp.float32
    ).astype(jnp.bfloat16)
    input_part = jnp.einsum(
        "secf,edf->secd", grad_pre_gate, w_gate, preferred_element_type=jnp.float32
    )
    input_part = input_part + jnp.einsum(
        "secf,edf->secd", grad_pre_up, w_up, preferred_element_type=jnp.float32
    )
    return (grad_gate, grad_up, grad_down, input_part)


def body_plain(
    stream_in,
    out_cot,
    route_experts,
    route_weights,
    w_gate,
    w_up,
    w_down,
    w_proj,
    conv_value,
    conv_gate,
    conv_taps,
    conv_result,
    channel_norm_gain,
):
    sp_count = lax.axis_size("sp")
    tp_count = lax.axis_size("tp")
    local_experts = w_gate.shape[0]
    experts_all = local_experts * sp_count
    token_rows, model_width = stream_in.shape
    top_count = route_experts.shape[1]
    capacity = 2 * top_count * token_rows // experts_all
    slot_of, source_of = slot_tables(route_experts, experts_all, capacity)
    occupied = source_of >= 0
    source_safe = jnp.maximum(source_of, 0)
    token_of = source_safe // top_count
    slot_weight = jnp.where(occupied, route_weights.reshape(-1)[source_safe], 0.0)
    row_buffer = jnp.where(occupied[:, None], stream_in[token_of], jnp.zeros((), jnp.bfloat16))
    cot_buffer = (slot_weight[:, None] * out_cot[token_of].astype(jnp.float32)).astype(jnp.bfloat16)
    row_buffer = row_buffer.reshape(experts_all, capacity, model_width)
    cot_buffer = cot_buffer.reshape(experts_all, capacity, model_width)
    slice_width = model_width // tp_count
    slice_start = lax.axis_index("tp") * slice_width
    row_slice = lax.dynamic_slice_in_dim(row_buffer, slice_start, slice_width, 2)
    cot_slice = lax.dynamic_slice_in_dim(cot_buffer, slice_start, slice_width, 2)
    row_slice, cot_slice = (
        lax.all_to_all(row_slice, "sp", split_axis=0, concat_axis=0, tiled=True),
        lax.all_to_all(cot_slice, "sp", split_axis=0, concat_axis=0, tiled=True),
    )
    rows_in, cot_in = (
        lax.all_gather(row_slice, "tp", axis=2, tiled=True),
        lax.all_gather(cot_slice, "tp", axis=2, tiled=True),
    )
    rows_in = rows_in.reshape(sp_count, local_experts, capacity, model_width)
    cot_in = cot_in.reshape(sp_count, local_experts, capacity, model_width)
    grad_gate, grad_up, grad_down, input_part = expert_terms_plain(rows_in, cot_in, w_gate, w_up, w_down)
    shared = lax.psum_scatter(
        input_part.astype(jnp.bfloat16), "tp", scatter_dimension=3, tiled=True
    )
    returned = shared.reshape(experts_all, capacity, slice_width)
    returned = lax.all_to_all(returned, "sp", split_axis=0, concat_axis=0, tiled=True)
    cot_cols = lax.dynamic_slice_in_dim(out_cot, slice_start, slice_width, 1)
    stream_part = combine_routes(returned, slot_of, cot_cols, token_rows, top_count)
    grad_stream = lax.all_gather(stream_part, "tp", axis=1, tiled=True)
    channel_total = conv_result.shape[0] * tp_count
    positions = conv_result.shape[1]
    conv_float = conv_result.astype(jnp.float32)
    chan_sum, chan_sq = lax.psum(
        (jnp.sum(conv_float, axis=0), jnp.sum(conv_float * conv_float, axis=0)), "tp"
    )
    chan_mean = chan_sum / channel_total
    chan_var = chan_sq / channel_total - chan_mean * chan_mean
    inverse_deviation = lax.rsqrt(chan_var + norm_eps)
    mean_removed = (conv_float - chan_mean) * inverse_deviation
    normalized_rows = mean_removed * channel_norm_gain[:, None]
    sigmoid_of_norm = jax.nn.sigmoid(normalized_rows)
    hidden = (normalized_rows * sigmoid_of_norm).astype(jnp.bfloat16)
    grad_proj = lax.psum_scatter(
        lax.dot_general(
            grad_stream, hidden, (((0,), (1,)), ((), ())), preferred_element_type=jnp.float32
        ),
        "sp",
        scatter_dimension=0,
        tiled=True,
    )
    hidden_gradient = lax.dot_general(
        w_proj, grad_stream, (((0,), (1,)), ((), ())), preferred_element_type=jnp.float32
    )
    normed_input_gradient = (
        hidden_gradient
        * sigmoid_of_norm
        * (1.0 + normalized_rows * (1.0 - sigmoid_of_norm))
        * channel_norm_gain[:, None]
    )
    average_products, cross_products = lax.psum(
        (
            jnp.sum(normed_input_gradient, axis=0),
            jnp.sum(normed_input_gradient * mean_removed, axis=0),
        ),
        "tp",
    )
    conv_output_gradient = inverse_deviation * (
        normed_input_gradient
        - average_products / channel_total
        - mean_removed * (cross_products / channel_total)
    )
    taps_count = conv_taps.shape[0]
    next_rim = from_behind(conv_output_gradient[:, : taps_count - 1], "sp", -1)
    extended = jnp.concatenate([conv_output_gradient, next_rim], axis=1)
    grad_gated = jnp.zeros_like(conv_output_gradient)
    for tap_index in range(taps_count):
        grad_gated = (
            grad_gated
            + conv_taps[tap_index][:, None] * extended[:, tap_index : tap_index + positions]
        )
    gate_sig = jax.nn.sigmoid(conv_gate.astype(jnp.float32))
    grad_value = (grad_gated * gate_sig).astype(jnp.bfloat16)
    grad_gate_in = (
        grad_gated * conv_value.astype(jnp.float32) * gate_sig * (1.0 - gate_sig)
    ).astype(jnp.bfloat16)
    return (grad_gate, grad_up, grad_down, grad_stream, grad_proj, grad_value, grad_gate_in)


def solution(mesh):
    return jax.shard_map(
        body if mesh.shape["tp"] == 4 else body_plain,
        mesh=mesh,
        in_specs=(
            P("sp", None),
            P("sp", None),
            P("sp", None),
            P("sp", None),
            P("sp", None, "tp"),
            P("sp", None, "tp"),
            P("sp", "tp", None),
            P(None, "tp"),
            P("tp", "sp"),
            P("tp", "sp"),
            P(None, "tp"),
            P("tp", "sp"),
            P("tp"),
        ),
        out_specs=(
            P("sp", None, "tp"),
            P("sp", None, "tp"),
            P("sp", "tp", None),
            P("sp", None),
            P("sp", "tp"),
            P("tp", "sp"),
            P("tp", "sp"),
        ),
        check_vma=False,
    )
```

profile of v0, /device:TPU:0, one launch (start us, length us, event | category | flops | bytes accessed | tf_op | source)
XLA Modules:
  0.0 106.6 jit_solution(1000961606898393555)
XLA Ops:
  0.6 0.0 copy-start
  0.6 0.0 copy-start.1
  0.7 1.2 %copy-done.1 = bf16[128,2048]{1,0:T(8,128)(2,1)S(1)} copy-done((bf16[128,2048]{1,0:T(8,128)(2,1)S(1)}, bf16[128,2048]{1,0:T(8,128)(2,1)}, u32[]{:S(2)}) %copy-start.1) | copy-done | bytes 524312
  1.8 0.0 copy-start.4
  1.8 1.0 copy-done.4
  2.9 0.0 copy-start.10
  2.9 0.7 copy-done.10
  3.6 0.0 copy-start.11
  3.6 0.7 copy-done.11
  4.2 39.1 %dispatch.1 = (bf16[512,2048]{1,0:T(8,128)(2,1)S(1)}, bf16[512,2048]{1,0:T(8,128)(2,1)S(1)}, bf16[512,128]{1,0:T(8,128)(2,1)S(1)}) custom-call(s32[2,128]{1,0:T(2,128)S(1)} %bitcast.35, f32[2,128]{1,0:T(2,128)S(1)} %bitcast.36, bf16[128,2048]{1,0:T(8,128)(2,1)S(1)} %copy-done.4, bf16[128,2048]{1,0:T(8,128)(2,1)S(1)} %copy-done.1), custom_call_target="tpu_custom_call" | custom-call | tf_op jit(solution)/shard_map/dispatch/pallas_call | solution.py:163
  43.3 2.8 %fusion.4 = f32[512,512]{1,0:T(8,128)S(1)} fusion(bf16[512,2048]{1,0:T(8,128)(2,1)S(1)} %get-tuple-element.18, bf16[1,2048,512]{2,1,0:T(8,128)(2,1)} %param.18), kind=kOutput, calls=%fused_computation.8 | convolution fusion | flops 1073741824 | bytes 5242880 | tf_op jit(solution)/shard_map/dot_general | solution.py:19
  46.2 0.0 copy-done
  46.2 0.0 copy-start.13
  46.2 1.2 %fusion.10 = f32[512,512]{1,0:T(8,128)S(1)} fusion(bf16[512,2048]{1,0:T(8,128)(2,1)S(1)} %get-tuple-element.18, bf16[1,2048,512]{2,1,0:T(8,128)(2,1)S(1)} %copy-done), kind=kOutput, calls=%fused_computation.14 | convolution fusion | flops 1073741824 | bytes 5242880 | tf_op jit(solution)/shard_map/dot_general | solution.py:19
  47.4 0.3 copy-done.13
  47.8 1.9 %select_convert_fusion = (bf16[512,512]{1,0:T(8,128)(2,1)S(1)}, bf16[512,512]{1,0:T(8,128)(2,1)S(1)}) fusion(f32[512,512]{1,0:T(8,128)S(1)} %fusion.4, f32[512,512]{1,0:T(8,128)S(1)} %fusion.10, bf16[512,2048]{1,0:T(8,128)(2,1)S(1)} %get-tuple-element.19, bf16[1,512,2048]{2,1,0:T(8,128)(2,1)S(1)} %copy-done.13), kind=kOutput, calls=%fused_computation.17 | convolution fusion | flops 1079508992 | bytes 7340032 | tf_op jit(solution)/shard_map/dot_general | solution.py:19
  49.7 2.8 %fusion.2 = bf16[1,512,2048]{2,1,0:T(8,128)(2,1)} fusion(bf16[512,2048]{1,0:T(8,128)(2,1)S(1)} %get-tuple-element.19, f32[512,512]{1,0:T(8,128)S(1)} %fusion.10, f32[512,512]{1,0:T(8,128)S(1)} %fusion.4), kind=kOutput, calls=%fused_computation.6 | convolution fusion | flops 1077411840 | bytes 6291456 | tf_op jit(solution)/shard_map/dot_general | solution.py:19
  52.5 2.6 %fusion.1 = bf16[1,2048,512]{2,1,0:T(8,128)(2,1)} fusion(bf16[512,2048]{1,0:T(8,128)(2,1)S(1)} %get-tuple-element.18, bf16[512,512]{1,0:T(8,128)(2,1)S(1)} %get-tuple-element.29), kind=kOutput, calls=%fused_computation.5 | convolution fusion | flops 1074790400 | bytes 4718592 | tf_op jit(solution)/shard_map/dot_general | solution.py:19
  55.1 2.6 %fusion = bf16[1,2048,512]{2,1,0:T(8,128)(2,1)} fusion(bf16[512,2048]{1,0:T(8,128)(2,1)S(1)} %get-tuple-element.18, bf16[512,512]{1,0:T(8,128)(2,1)S(1)} %get-tuple-element.30), kind=kOutput, calls=%fused_computation.4 | convolution fusion | flops 1074790400 | bytes 4718592 | tf_op jit(solution)/shard_map/dot_general | solution.py:19
  57.7 0.0 copy-start.12
  57.7 1.3 %fusion.8 = f32[512,2048]{1,0:T(8,128)S(1)} fusion(bf16[512,512]{1,0:T(8,128)(2,1)S(1)} %get-tuple-element.30, bf16[1,2048,512]{2,1,0:T(8,128)(2,1)S(1)} %copy-done), kind=kOutput, calls=%fused_computation.12 | convolution fusion | flops 1073741824 | bytes 6815744 | tf_op jit(solution)/shard_map/dot_general | solution.py:19
  59.0 0.3 copy-done.12
  59.3 0.0 copy-start.2
  59.3 0.0 copy-start.3
  59.3 0.0 copy-start.5
  59.3 0.0 copy-start.6
  59.3 0.0 copy-start.7
  59.3 0.0 copy-start.8
  59.3 0.0 copy-start.9
  59.4 1.3 %add_convert_fusion.part_ref = bf16[512,2048]{1,0:T(8,128)(2,1)S(1)} fusion(f32[512,2048]{1,0:T(8,128)S(1)} %fusion.8, bf16[512,512]{1,0:T(8,128)(2,1)S(1)} %get-tuple-element.29, bf16[1,2048,512]{2,1,0:T(8,128)(2,1)S(1)} %copy-done.12), kind=kOutput, calls=%fused_computation | convolution fusion | flops 1075838976 | bytes 8912896 | tf_op jit(solution)/shard_map/dot_general | solution.py:19
  60.7 0.0 copy-done.2
  60.7 0.0 copy-done.3
  60.7 0.0 copy-done.5
  60.7 0.0 copy-done.6
  60.7 0.0 copy-done.7
  60.7 0.0 copy-done.8
  60.7 0.0 copy-done.9
  60.7 44.9 %combine_tail.1 = (bf16[128,2048]{1,0:T(8,128)(2,1)S(1)}, f32[256,256]{1,0:T(8,128)S(1)}, bf16[256,128]{1,0:T(8,128)(2,1)S(1)}, bf16[256,128]{1,0:T(8,128)(2,1)S(1)}) custom-call(bf16[512,2048]{1,0:T(8,128)(2,1)S(1)} %add_convert_fusion.part_ref, bf16[512,128]{1,0:T(8,128)(2,1)S(1)} %get-tuple-element.20.pick_ref, bf16[128,2048]{1,0:T(8,128)(2,1)S(1)} %copy-done.2, ...), custom_call_target="tpu_custom_call" | custom-call | tf_op jit(solution)/shard_map/combine_tail/pallas_call | solution.py:409
  105.6 0.9 flush.1
Async XLA Ops:
  0.6 45.5 %copy-start = (bf16[1,2048,512]{2,1,0:T(8,128)(2,1)S(1)}, bf16[1,2048,512]{2,1,0:T(8,128)(2,1)}, u32[]{:S(2)}) copy-start(bf16[1,2048,512]{2,1,0:T(8,128)(2,1)} %param.17) | copy-start | bytes 6291460
  0.6 1.2 %copy-start.1 = (bf16[128,2048]{1,0:T(8,128)(2,1)S(1)}, bf16[128,2048]{1,0:T(8,128)(2,1)}, u32[]{:S(2)}) copy-start(bf16[128,2048]{1,0:T(8,128)(2,1)} %cot_ref.3) | copy-start | bytes 1572868
  1.8 1.0 copy-start.4
  2.9 0.7 copy-start.10
  3.6 0.7 copy-start.11
  46.2 1.6 %copy-start.13 = (bf16[1,512,2048]{2,1,0:T(8,128)(2,1)S(1)}, bf16[1,512,2048]{2,1,0:T(8,128)(2,1)}, u32[]{:S(2)}) copy-start(bf16[1,512,2048]{2,1,0:T(8,128)(2,1)} %param.19) | copy-start | bytes 6291460
  57.7 1.6 %copy-start.12 = (bf16[1,2048,512]{2,1,0:T(8,128)(2,1)S(1)}, bf16[1,2048,512]{2,1,0:T(8,128)(2,1)}, u32[]{:S(2)}) copy-start(bf16[1,2048,512]{2,1,0:T(8,128)(2,1)} %param.18) | copy-start | bytes 6291460
  59.3 1.3 %copy-start.2 = (bf16[128,2048]{1,0:T(8,128)(2,1)S(1)}, bf16[128,2048]{1,0:T(8,128)(2,1)}, u32[]{:S(2)}) copy-start(bf16[128,2048]{1,0:T(8,128)(2,1)} %cot_ref.3) | copy-start | bytes 1572868
  59.3 1.4 %copy-start.3 = (bf16[2048,256]{1,0:T(8,128)(2,1)S(1)}, bf16[2048,256]{1,0:T(8,128)(2,1)}, u32[]{:S(2)}) copy-start(bf16[2048,256]{1,0:T(8,128)(2,1)} %proj_ref.1) | copy-start | bytes 3145732
  59.3 1.4 %copy-start.5 = (bf16[256,128]{1,0:T(8,128)(2,1)S(1)}, bf16[256,128]{1,0:T(8,128)(2,1)}, u32[]{:S(2)}) copy-start(bf16[256,128]{1,0:T(8,128)(2,1)} %value_ref.1) | copy-start | bytes 196612
  59.3 1.4 %copy-start.6 = (bf16[256,128]{1,0:T(8,128)(2,1)S(1)}, bf16[256,128]{1,0:T(8,128)(2,1)}, u32[]{:S(2)}) copy-start(bf16[256,128]{1,0:T(8,128)(2,1)} %gate_ref.1) | copy-start | bytes 196612
  59.3 1.4 %copy-start.7 = (bf16[256,128]{1,0:T(8,128)(2,1)S(1)}, bf16[256,128]{1,0:T(8,128)(2,1)}, u32[]{:S(2)}) copy-start(bf16[256,128]{1,0:T(8,128)(2,1)} %conv_ref.1) | copy-start | bytes 196612
  59.3 1.4 %copy-start.8 = (f32[31,256]{1,0:T(8,128)S(1)}, f32[31,256]{1,0:T(8,128)}, u32[]{:S(2)}) copy-start(f32[31,256]{1,0:T(8,128)} %taps_ref.1) | copy-start | bytes 95236
  59.3 1.4 %copy-start.9 = (f32[256]{0:T(256)S(1)}, f32[256]{0:T(256)}, u32[]{:S(2)}) copy-start(f32[256]{0:T(256)} %param.25) | copy-start | bytes 3076
where the time goes:
time: 107 us
  Pallas kernels  84.9 us (79%)
  matrix products  16.6 us (16%)
  local copies, waits for them, and re-layouts  4.28 us (4%)
    pallas_call x1, Pallas kernels, tail(): pl.pallas_call(functools.partial(tail_kernel, n, cap, channels * tp_count...  44.9 us
    pallas_call x1, Pallas kernels, dispatch(): pl.pallas_call(functools.partial(dispatch_kernel, n, cap), out_shape=(jax...  39.1 us
    dot_general x8, matrix products, dot(): lax.dot_general(a, b, (((ca,), (cb,)), ((), ())), preferred_element_type=...  16.6 us
    unnamed x28, local copies, waits for them, and re-layouts  4.28 us

commit v1 on v0

v1 whole, which is shorter than its diff:
```python
import functools

import jax
import jax.numpy as jnp
from jax import lax
from jax.experimental import pallas as pl
from jax.experimental.pallas import tpu as pltpu
from jax.sharding import PartitionSpec as P

norm_eps = 1e-05
clamp_limit = 7.0
alpha_gate = 1.702
MESH = pl.DeviceIdType.MESH
f32 = jnp.float32
bf16 = jnp.bfloat16


def dot(a, b, ca=1, cb=0):
    return lax.dot_general(a, b, (((ca,), (cb,)), ((), ())), preferred_element_type=f32)


def aligned(start, size):
    return pl.ds(pl.multiple_of(start, size), size)


def greet(n, s, q, tp_peers):
    barrier = pltpu.get_barrier_semaphore()
    for d in range(1, n):
        pl.semaphore_signal(
            barrier, inc=1, device_id={"sp": lax.rem(s + d, n), "tp": q}, device_id_type=MESH
        )
    for peer in tp_peers:
        pl.semaphore_signal(barrier, inc=1, device_id={"sp": s, "tp": peer}, device_id_type=MESH)
    pl.semaphore_wait(barrier, n - 1 + len(tp_peers))


def remote(src, dst, send, recv, sp, tp):
    return pltpu.make_async_remote_copy(
        src_ref=src,
        dst_ref=dst,
        send_sem=send,
        recv_sem=recv,
        device_id={"sp": sp, "tp": tp},
        device_id_type=MESH,
    )


def partners(q):
    core, other = lax.rem(q, 2), q // 2
    return (2 * other + 1 - core, 2 * (1 - other) + core, 2 * (1 - other) + 1 - core)


def slot_pick(routes, weights, first, slots, cap):
    top, tokens = routes.shape
    local = routes - first
    expert_ids = lax.broadcasted_iota(jnp.int32, (8, tokens), 0)
    hits = [expert_ids == local[k : k + 1, :] for k in range(top)]
    count = sum(h.astype(f32) for h in hits)
    earlier = (
        lax.broadcasted_iota(jnp.int32, (tokens, tokens), 0)
        < lax.broadcasted_iota(jnp.int32, (tokens, tokens), 1)
    ).astype(f32)
    before = dot(count.astype(bf16), earlier.astype(bf16))
    slot_ids = lax.broadcasted_iota(jnp.int32, (slots, tokens), 0)
    pick = jnp.zeros((slots, tokens), f32)
    weighted = jnp.zeros((slots, tokens), f32)
    for k in range(top):
        rank = jnp.sum(jnp.where(hits[k], before, 0.0), axis=0, keepdims=True)
        here = slot_ids == local[k : k + 1, :] * cap + rank.astype(jnp.int32)
        pick = jnp.where(here, 1.0, pick)
        weighted = jnp.where(here, weights[k : k + 1, :], weighted)
    return pick.astype(bf16), jnp.sum(weighted, axis=1, keepdims=True)


def fused_kernel(n, cap, channel_total, names, *refs):
    r = dict(zip(names, refs))
    s, q = lax.axis_index("sp"), lax.axis_index("tp")
    q_core, q_y, q_far = partners(q)
    peers = (q_core, q_y, q_far)
    core, y = lax.rem(q, 2), q // 2
    z, x = s // 2, lax.rem(s, 2)
    sx = s + 1 - 2 * x
    nz = n // 2
    stream, cot = r["stream"], r["cot"]
    tokens, model_width = stream.shape
    width = r["ret"].shape[-1]
    top = r["routes"].shape[0]
    icols = r["gproj"].shape[0]
    pair = 2 * cap
    taps_count = r["taps"].shape[0]
    quarter, quarter_y = aligned(q * width, width), aligned(q_y * width, width)
    wg, wu, wd = r["wg"], r["wu"], r["wd"]
    full = (r["rows"], r["cots"])
    copies = []
    conditional = []

    loads = {}
    for i, name in enumerate(input_names):
        loads[name] = pltpu.make_async_copy(r[name + "_h"], r[name], r["load"].at[i])
        loads[name].start()

    def start(src, dst, key, index, sp, tp, recv=None):
        send, arrive = r["send_" + key], r["recv_" + key]
        copy = remote(src, dst, send.at[index], arrive.at[index if recv is None else recv], sp, tp)
        copy.start()
        copies.append(copy)
        return copy

    def start_if(cond, src, dst, key, index, sp, tp, recv):
        copy = remote(
            src, dst, r["send_" + key].at[index], r["recv_" + key].at[recv], sp, tp
        )
        pl.when(cond)(copy.start)
        conditional.append((cond, copy))

    def landed(dst, key, index):
        remote(dst, dst, r["send_" + key].at[index], r["recv_" + key].at[index], s, q).wait_recv()

    high = z // (nz // 2)
    folded = z + high * (nz - 1 - 2 * z)
    far_order = [1 - folded, 2 + 0 * z, 3 + 0 * z]
    source = [f + high * (nz - 1 - 2 * f) for f in far_order]
    chunk_z = [z] + source
    chunk_rows = [aligned(c * pair, pair) for c in chunk_z]

    def block_rows(block):
        return aligned(block * cap, cap)

    loads["routes"].wait()
    loads["weights"].wait()
    meta = r["meta"]
    routes_own, weights_own = r["routes"][...], r["weights"][...]
    meta[z] = jnp.concatenate(
        [routes_own.astype(f32), weights_own, jnp.zeros((8 - 2 * top, tokens), f32)], axis=0
    )
    greet(n, s, q, peers)
    meta_waits = [
        start(meta.at[z], meta.at[z], "m", d - 1, 2 * lax.rem(z + d, nz) + x, q)
        for d in range(1, nz)
    ]
    raw = r["raw"]
    values = (stream, cot)
    for a, name in enumerate(("stream", "cot")):
        loads[name].wait()
        src = values[a].at[:, quarter]
        start_if(z < nz - 1, src, raw.at[a, z], "zo", (a, 0), s + 2, q, (a, z))
        start_if(z > 0, src, raw.at[a, z], "zp", (a, 0), s - 2, q, (a, z))

    def landed_raw(a, j):
        dst = raw.at[a, source[j]]
        from_below = source[j] < z

        @pl.when(from_below)
        def _():
            landed(dst, "zo", (a, source[j]))

        @pl.when(source[j] > z)
        def _():
            landed(dst, "zp", (a, source[j]))

        start_if((source[j] < z) & (z < nz - 1), dst, dst, "zo", (a, j + 1), s + 2, q, (a, source[j]))
        start_if((source[j] > z) & (z > 0), dst, dst, "zp", (a, j + 1), s - 2, q, (a, source[j]))

    pick, slot_weight = slot_pick(routes_own, weights_own, 2 * z, pair, cap)
    ownbuf = r["ownbuf"]
    own_half, other_half = aligned(x * cap, cap), aligned((1 - x) * cap, cap)
    for a in range(2):
        got = dot(pick, values[a][...])
        ownbuf[a] = (got * slot_weight if a else got).astype(bf16)
        for i, cols in enumerate((quarter, quarter_y)):
            start(
                ownbuf.at[a, other_half, cols], full[a].at[block_rows(s), cols],
                "xo", (a, i), sx, q,
            )
    for a in range(2):
        full[a][block_rows(s), :] = ownbuf[a, own_half, :]
    r["pick"][...] = slot_pick(routes_own, weights_own, 0, n * cap, cap)[0]

    def exchange_stats(buffer, first, second, which):
        lanes = lax.broadcasted_iota(jnp.int32, (tokens, tokens), 1)
        packed = jnp.where(lanes == 0, first, jnp.where(lanes == 1, second, 0.0))
        buffer[3] = packed.T[0:8, :]
        return [
            start(buffer.at[3], buffer.at[p], "s", (which, p), s, peer)
            for p, peer in enumerate(peers)
        ]

    def summed_stats(buffer, waits):
        for w in waits:
            w.wait_recv()
        total = (buffer[3] + buffer[0]) + (buffer[1] + buffer[2])
        wide = jnp.concatenate([total, jnp.zeros((tokens - 8, tokens), f32)], axis=0).T
        return wide[:, 0:1], wide[:, 1:2]

    loads["conv"].wait()
    loads["gain"].wait()
    conv = r["conv"][...].astype(f32).T
    stat_waits = exchange_stats(
        r["stat"],
        jnp.sum(conv, axis=1, keepdims=True),
        jnp.sum(conv * conv, axis=1, keepdims=True),
        0,
    )
    for copy in meta_waits:
        copy.wait_recv()
    picks = []
    for j in range(nz - 1):
        there = meta[source[j]]
        picks.append(
            slot_pick(there[0:top].astype(jnp.int32), there[top : 2 * top], 2 * z, pair, cap)
        )
    pickbuf = r["pickbuf"]

    def arrive_raw(j, a):
        landed_raw(a, j)
        pick_j, weight_j = picks[j]
        got = dot(pick_j, raw[a, source[j]])
        pickbuf[a, j] = (got * weight_j if a else got).astype(bf16)
        rows = block_rows(2 * source[j] + x)
        mine, other = pickbuf.at[a, j, own_half], pickbuf.at[a, j, other_half]
        here = full[a].at[rows, quarter]
        start(other, here, "x", (a, j), sx, q)
        start(mine, here, "y", (a, j, 0), s, q_y)
        start(mine, here, "c", (a, j, 0), s, q_core)
        full[a][rows, quarter] = pickbuf[a, j, own_half]

    def arrive_x(j, a):
        here = full[a].at[block_rows(2 * source[j] + 1 - x), quarter]
        landed(here, "x", (a, j))
        start(here, here, "y", (a, j, 1), s, q_y)
        start(here, here, "c", (a, j, 1), s, q_core)

    def arrive_y(j, a):
        for i in range(2):
            here = full[a].at[block_rows(2 * source[j] + (x if i == 0 else 1 - x)), quarter_y]
            landed(here, "y", (a, j, i))
            start(here, here, "d", (a, j, i), s, q_core)

    def complete(j, a):
        for i in range(2):
            rows = block_rows(2 * source[j] + (x if i == 0 else 1 - x))
            for key, owner in (("c", q_core), ("d", q_far)):
                landed(full[a].at[rows, aligned(owner * width, width)], key, (a, j, i))

    def arrive_own(a):
        for i, cols in enumerate((quarter, quarter_y)):
            here = full[a].at[block_rows(sx), cols]
            landed(here, "xo", (a, i))
            start(here, here, "xc", (a, i), s, q_core)

    def complete_own(a):
        for i, owner in enumerate((q_core, q_far)):
            landed(full[a].at[block_rows(sx), aligned(owner * width, width)], "xc", (a, i))

    act_all, dg_all, du_all, part = r["act"], r["dg"], r["du"], r["part"]
    pre_gate_ref, pre_up_ref = r["pre_gate"], r["pre_up"]

    def first_half(k):
        rows = chunk_rows[k]
        if k:
            complete(k - 1, 0)
        else:
            complete_own(0)
            loads["wg"].wait()
            loads["wu"].wait()
        rows_in = full[0][rows, :]
        pre_gate_ref[...] = dot(rows_in, wg[...])
        pre_up_ref[...] = dot(rows_in, wu[...])

    def second_half(k):
        rows = chunk_rows[k]
        if k:
            complete(k - 1, 1)
        else:
            complete_own(1)
            loads["wd"].wait()
        grad_act = dot(full[1][rows, :], wd[...], 1, 1)
        pre_gate, pre_up = pre_gate_ref[...], pre_up_ref[...]
        glu_part = jnp.minimum(pre_gate, clamp_limit)
        lin_part = jnp.clip(pre_up, -clamp_limit, clamp_limit)
        sig_glu = jax.nn.sigmoid(alpha_gate * glu_part)
        act_all[rows, :] = (glu_part * sig_glu * (lin_part + 1.0)).astype(bf16)
        slope = sig_glu + alpha_gate * glu_part * sig_glu * (1.0 - sig_glu)
        dg = jnp.where(
            pre_gate < clamp_limit, grad_act * (lin_part + 1.0) * slope, 0.0
        ).astype(bf16)
        du = jnp.where(
            jnp.abs(pre_up) < clamp_limit, grad_act * glu_part * sig_glu, 0.0
        ).astype(bf16)
        dg_all[rows, :] = dg
        du_all[rows, :] = du
        part[rows, :] = (dot(dg, wg[...], 1, 1) + dot(du, wu[...], 1, 1)).astype(bf16)
        for h, half in ((0, 1 - y), (1, y)):
            start(
                part.at[rows, aligned((2 * half + 1 - core) * width, width)],
                r["from_core"].at[h, rows], "rc", (k, h), s, q_core,
            )

    def reduce_core(k):
        rows = chunk_rows[k]
        landed(r["from_core"].at[0, rows], "rc", (k, 0))
        r["to_y"][rows, :] = (
            part[rows, quarter_y].astype(f32) + r["from_core"][0, rows, :].astype(f32)
        ).astype(bf16)
        start(r["to_y"].at[rows], r["from_y"].at[rows], "ry", k, s, q_y)
        landed(r["from_core"].at[1, rows], "rc", (k, 1))
        r["own"][rows, :] = part[rows, quarter].astype(f32) + r["from_core"][
            1, rows, :
        ].astype(f32)

    ret = r["ret"]
    mine_slots = block_rows(s)

    def reduce_y(k):
        rows = chunk_rows[k]
        landed(r["from_y"].at[rows], "ry", k)
        r["to_xz"][rows, :] = (
            r["own"][rows, :] + r["from_y"][rows, :].astype(f32)
        ).astype(bf16)
        if k:
            for i in range(2):
                home = 2 * chunk_z[k] + i
                start(r["to_xz"].at[block_rows(home)], ret.at[mine_slots], "r", (k, i), home, q, (s, 0))
        else:
            start(r["to_xz"].at[block_rows(sx)], ret.at[mine_slots], "r", (0, 0), sx, q, (s, 0))
            ret[mine_slots, :] = r["to_xz"][mine_slots, :]

    hid_all = r["hid"]

    def hid_rows(block):
        return aligned(block * tokens, tokens)

    def relay_hidden(j):
        if j < 0:
            here = hid_all.at[hid_rows(s)]
            start_if(z < nz - 1, here, here, "ho", 0, s + 2, q, z)
            start_if(z > 0, here, here, "hp", 0, s - 2, q, z)
        else:
            here = hid_all.at[hid_rows(2 * source[j] + x)]

            @pl.when(source[j] < z)
            def _():
                landed(here, "ho", source[j])

            @pl.when(source[j] > z)
            def _():
                landed(here, "hp", source[j])

            start_if((source[j] < z) & (z < nz - 1), here, here, "ho", j + 1, s + 2, q, source[j])
            start_if((source[j] > z) & (z > 0), here, here, "hp", j + 1, s - 2, q, source[j])
        start(here, here, "hx", j + 1, sx, q)

    def weight_grad(left, right, out, by_left):
        tile = right.shape[1] if by_left else left.shape[1]

        def step(i, carry):
            there = aligned(i * tile, tile)
            if by_left:
                out[there, :] = dot(left[:, there], right[...], 0, 0).astype(bf16)
            else:
                out[:, there] = dot(left[...], right[:, there], 0, 0).astype(bf16)
            return carry

        lax.fori_loop(0, model_width // tile, step, 0)

    arrive_raw(0, 0)
    arrive_own(0)
    chan_sum, chan_sq = summed_stats(r["stat"], stat_waits)
    chan_mean = chan_sum / channel_total
    chan_var = chan_sq / channel_total - chan_mean * chan_mean
    inverse_deviation = lax.rsqrt(chan_var + norm_eps)
    mean_removed = (conv - chan_mean) * inverse_deviation
    gain = r["gain"][...]
    normed = mean_removed * gain
    sig = jax.nn.sigmoid(normed)
    hid_all[hid_rows(s), :] = (normed * sig).astype(bf16)
    r["slope"][...] = sig * (1.0 + normed * (1.0 - sig)) * gain
    r["removed"][...] = mean_removed
    r["inverse"][...] = jnp.broadcast_to(inverse_deviation, r["inverse"].shape)
    arrive_raw(0, 1)
    arrive_own(1)
    arrive_x(0, 0)
    first_half(0)
    arrive_raw(1, 0)
    arrive_y(0, 0)
    arrive_x(0, 1)
    second_half(0)
    arrive_raw(1, 1)
    arrive_y(0, 1)
    arrive_x(1, 0)
    first_half(1)
    arrive_raw(2, 0)
    arrive_y(1, 0)
    arrive_x(1, 1)
    second_half(1)
    arrive_raw(2, 1)
    relay_hidden(-1)
    arrive_y(1, 1)
    arrive_x(2, 0)
    reduce_core(0)
    first_half(2)
    arrive_x(2, 1)
    arrive_y(2, 0)
    second_half(2)
    reduce_core(1)
    arrive_y(2, 1)
    first_half(3)
    second_half(3)
    reduce_y(0)
    reduce_core(2)
    reduce_core(3)
    relay_hidden(0)
    reduce_y(1)
    weight_grad(r["act"], r["cots"], r["gdown"], False)
    reduce_y(2)
    relay_hidden(1)
    reduce_y(3)
    relay_hidden(2)
    weight_grad(r["rows"], r["dg"], r["ggate"], True)
    weight_grad(r["rows"], r["du"], r["gup"], True)

    for d in range(1, n):
        e = lax.rem(s + d, n)
        landed(ret.at[block_rows(e)], "r", (e, 0))
    gs_ref = r["gs"]
    combined = dot(r["pick"][...], ret[...], 0, 0) + cot[:, quarter].astype(f32)
    gs_ref[:, quarter] = combined.astype(bf16)
    mine_cols = gs_ref.at[:, quarter]
    by_core = start(mine_cols, mine_cols, "g", 0, s, q_core)
    by_y = start(mine_cols, mine_cols, "g", 1, s, q_y)
    loads["proj"].wait()
    proj = r["proj"]

    def partial_of(owner):
        cols = aligned(owner * width, width)
        return dot(gs_ref[:, cols], proj[cols, :])

    grad_hidden = partial_of(q)
    by_y.wait_recv()
    y_cols = gs_ref.at[:, quarter_y]
    by_far = start(y_cols, y_cols, "g", 2, s, q_core)
    grad_hidden = grad_hidden + partial_of(q_y)
    by_core.wait_recv()
    grad_hidden = grad_hidden + partial_of(q_core)
    by_far.wait_recv()
    grad_hidden = grad_hidden + partial_of(q_far)
    half_rows = tokens // 2
    part_rows = aligned(core * half_rows, half_rows)
    land = aligned(s * tokens + core * half_rows, half_rows)
    order = [lax.rem(s + d, n) for d in range(1, n)]
    col_all = r["col"]
    col_waits = [
        start(
            gs_ref.at[part_rows, aligned(order[j] * icols, icols)], col_all.at[land],
            "k", j, order[j], q,
        )
        for j in range(n - 1)
    ]
    col_all[hid_rows(s), :] = gs_ref[:, aligned(s * icols, icols)]
    mean_removed = r["removed"][...]
    inverse_deviation = r["inverse"][:, 0:1]
    norm_grad = grad_hidden * r["slope"][...]
    stat_waits = exchange_stats(
        r["stat2"],
        jnp.sum(norm_grad, axis=1, keepdims=True),
        jnp.sum(norm_grad * mean_removed, axis=1, keepdims=True),
        1,
    )
    avg, cross = summed_stats(r["stat2"], stat_waits)
    conv_grad = inverse_deviation * (
        norm_grad - avg / channel_total - mean_removed * (cross / channel_total)
    )
    ext = r["ext"]
    rim = ext.shape[0] - tokens
    ext[0:tokens, :] = conv_grad
    halo = remote(
        ext.at[0:rim], ext.at[tokens : tokens + rim], r["send_e"].at[0], r["recv_e"].at[0],
        lax.rem(s + n - 1, n), q,
    )
    halo.start()
    forwards = []
    for j in range(n - 1):
        col_waits[j].wait_recv()
        origin = lax.rem(s + n - (j + 1), n)
        there = col_all.at[aligned(origin * tokens + core * half_rows, half_rows)]
        forwards.append(start(there, there, "f", j, s, q_core))
    loads["taps"].wait()
    loads["gate"].wait()
    loads["value"].wait()
    halo.wait_recv()
    edge = ext[tokens : tokens + rim, :]
    halo.wait_send()
    ext[tokens : tokens + rim, :] = jnp.where(s == n - 1, 0.0, edge)
    acc = jnp.zeros((tokens, ext.shape[1]), f32)
    for tap in range(taps_count):
        acc = acc + r["taps"][tap : tap + 1, :] * ext[tap : tap + tokens, :]
    gated = acc.T
    gate_sig = jax.nn.sigmoid(r["gate"][...].astype(f32))
    r["gvalue"][...] = (gated * gate_sig).astype(bf16)
    r["ggin"][...] = (
        gated * r["value"][...].astype(f32) * gate_sig * (1.0 - gate_sig)
    ).astype(bf16)
    for copy in forwards:
        copy.wait_recv()
    for k in range(nz):
        landed(hid_all.at[hid_rows(2 * chunk_z[k] + 1 - x)], "hx", k)
    r["gproj"][...] = dot(col_all[...], hid_all[...], 0, 0)
    for copy in copies:
        copy.wait_send()
    for cond, copy in conditional:
        pl.when(cond)(copy.wait_send)


input_names = (
    "routes", "weights", "stream", "cot", "conv", "gain", "wg", "wu", "wd", "proj", "value",
    "gate", "taps",
)


def fused(
    routes, weights, stream, cot, wg, wu, wd, proj, value, gate, taps, conv, gain, n, cap, tp_count
):
    tokens, model_width = stream.shape
    hidden_width = wg.shape[1]
    width = model_width // tp_count
    channels = value.shape[0]
    icols = model_width // n
    slots = n * cap
    rim = -(-(taps.shape[0] - 1) // 8) * 8
    nz = n // 2
    V, dma = pltpu.VMEM, pltpu.SemaphoreType.DMA
    given = dict(
        routes=routes, weights=weights, stream=stream, cot=cot, conv=conv, gain=gain, wg=wg, wu=wu,
        wd=wd, proj=proj, value=value, gate=gate, taps=taps,
    )
    outs = dict(
        ggate=((model_width, hidden_width), bf16),
        gup=((model_width, hidden_width), bf16),
        gdown=((hidden_width, model_width), bf16),
        gs=((tokens, model_width), bf16),
        gproj=((icols, channels), f32),
        gvalue=((channels, tokens), bf16),
        ggin=((channels, tokens), bf16),
    )
    scratch = {name: V(given[name].shape, given[name].dtype) for name in input_names}
    scratch.update(
        meta=V((nz, 8, tokens), f32),
        raw=V((2, nz, tokens, width), bf16),
        ownbuf=V((2, 2 * cap, model_width), bf16),
        pickbuf=V((2, nz - 1, 2 * cap, width), bf16),
        pick=V((slots, tokens), bf16),
        rows=V((slots, model_width), bf16),
        cots=V((slots, model_width), bf16),
        act=V((slots, hidden_width), bf16),
        dg=V((slots, hidden_width), bf16),
        du=V((slots, hidden_width), bf16),
        part=V((slots, model_width), bf16),
        pre_gate=V((2 * cap, hidden_width), f32),
        pre_up=V((2 * cap, hidden_width), f32),
        from_core=V((2, slots, width), bf16),
        own=V((slots, width), f32),
        to_y=V((slots, width), bf16),
        from_y=V((slots, width), bf16),
        to_xz=V((slots, width), bf16),
        ret=V((slots, width), bf16),
        hid=V((n * tokens, channels), bf16),
        col=V((n * tokens, icols), bf16),
        slope=V((tokens, channels), f32),
        removed=V((tokens, channels), f32),
        inverse=V((tokens, tokens), f32),
        stat=V((4, 8, tokens), f32),
        stat2=V((4, 8, tokens), f32),
        ext=V((tokens + rim, channels), f32),
        load=dma((len(input_names),)),
    )
    sems = dict(
        m=(nz - 1,), zo=(2, nz), zp=(2, nz), xo=(2, 2), xc=(2, 2), x=(2, nz - 1), y=(2, nz - 1, 2),
        c=(2, nz - 1, 2), d=(2, nz - 1, 2), s=(2, 3), rc=(nz, 2), ry=(nz,), ho=(nz,), hp=(nz,),
        hx=(nz,), g=(3,), k=(n - 1,), f=(n - 1,), e=(1,), r=(n, 2),
    )
    for key, shape in sems.items():
        scratch["send_" + key] = dma(shape)
        scratch["recv_" + key] = dma(shape)
    names = [name + "_h" for name in input_names] + list(outs) + list(scratch)
    return pl.pallas_call(
        functools.partial(fused_kernel, n, cap, channels * tp_count, tuple(names)),
        out_shape=tuple(jax.ShapeDtypeStruct(*o) for o in outs.values()),
        in_specs=[pl.BlockSpec(memory_space=pltpu.HBM)] * len(input_names),
        out_specs=[pl.BlockSpec(memory_space=V)] * len(outs),
        scratch_shapes=list(scratch.values()),
        compiler_params=pltpu.CompilerParams(
            collective_id=0, has_side_effects=True, vmem_limit_bytes=48 << 20
        ),
        name="fused",
    )(*[given[name] for name in input_names])


def flush_kernel(*refs):
    count = len(refs) // 2
    copies = [
        pltpu.make_async_copy(refs[i], refs[count + i], refs[-1].at[i]) for i in range(count)
    ]
    for copy in copies:
        copy.start()
    for copy in copies:
        copy.wait()


def flush(*arrays):
    return pl.pallas_call(
        flush_kernel,
        out_shape=tuple(jax.ShapeDtypeStruct(a.shape, a.dtype) for a in arrays),
        in_specs=[pl.BlockSpec(memory_space=pltpu.VMEM)] * len(arrays),
        out_specs=[pl.BlockSpec(memory_space=pltpu.HBM)] * len(arrays),
        scratch_shapes=[pltpu.SemaphoreType.DMA((len(arrays),))],
        compiler_params=pltpu.CompilerParams(vmem_limit_bytes=4 << 20),
        name="flush",
    )(*arrays)


def body(
    stream_in, out_cot, route_experts, route_weights, w_gate, w_up, w_down, w_proj,
    conv_value, conv_gate, conv_taps, conv_result, channel_norm_gain,
):
    n = lax.axis_size("sp")
    tp_count = lax.axis_size("tp")
    experts = w_gate.shape[0] * n
    tokens, model_width = stream_in.shape
    cap = 2 * route_experts.shape[1] * tokens // experts
    outs = flush(
        *fused(
            route_experts.T, route_weights.T, stream_in, out_cot, w_gate[0], w_up[0], w_down[0],
            w_proj, conv_value, conv_gate, conv_taps, conv_result, channel_norm_gain[None, :],
            n, cap, tp_count,
        )
    )
    return (outs[0][None], outs[1][None], outs[2][None]) + tuple(outs[3:])


def from_behind(value, axis, steps):
    count = lax.axis_size(axis)
    leading, last = (max(0, -steps), min(count, count - steps))
    return lax.ppermute(value, axis, [(source, source + steps) for source in range(leading, last)])


def slot_tables(block_routes, experts_all, capacity):
    flat_routes = block_routes.reshape(-1)
    assigns = flat_routes.shape[0]
    onehot = (flat_routes[:, None] == jnp.arange(experts_all, dtype=jnp.int32)[None, :]).astype(
        jnp.int32
    )
    before = jnp.cumsum(onehot, axis=0) - onehot
    rank_in = jnp.sum(before * onehot, axis=1)
    slot_of = flat_routes * capacity + rank_in
    source_of = (
        jnp.full((experts_all * capacity,), -1, jnp.int32)
        .at[slot_of]
        .set(jnp.arange(assigns, dtype=jnp.int32))
    )
    return (slot_of, source_of)


def combine_routes(returned, slot_of, cot_cols, token_rows, top_count):
    feature_count = returned.shape[-1]
    flat_back = returned.reshape(-1, feature_count)
    per_route = flat_back[slot_of].astype(jnp.float32).reshape(token_rows, top_count, feature_count)
    return (cot_cols.astype(jnp.float32) + jnp.sum(per_route, axis=1)).astype(jnp.bfloat16)


def expert_terms_plain(rows_in, cot_in, w_gate, w_up, w_down):
    pre_gate = jnp.einsum("secd,edf->secf", rows_in, w_gate, preferred_element_type=jnp.float32)
    pre_up = jnp.einsum("secd,edf->secf", rows_in, w_up, preferred_element_type=jnp.float32)
    glu_part = jnp.minimum(pre_gate, clamp_limit)
    lin_part = jnp.clip(pre_up, -clamp_limit, clamp_limit)
    sig_glu = jax.nn.sigmoid(alpha_gate * glu_part)
    activated = (glu_part * sig_glu * (lin_part + 1.0)).astype(jnp.bfloat16)
    grad_act = jnp.einsum("secd,efd->secf", cot_in, w_down, preferred_element_type=jnp.float32)
    slope = sig_glu + alpha_gate * glu_part * sig_glu * (1.0 - sig_glu)
    grad_pre_gate = jnp.where(
        pre_gate < clamp_limit, grad_act * (lin_part + 1.0) * slope, 0.0
    ).astype(jnp.bfloat16)
    grad_pre_up = jnp.where(
        jnp.abs(pre_up) < clamp_limit, grad_act * glu_part * sig_glu, 0.0
    ).astype(jnp.bfloat16)
    grad_down = jnp.einsum(
        "secf,secd->efd", activated, cot_in, preferred_element_type=jnp.float32
    ).astype(jnp.bfloat16)
    grad_gate = jnp.einsum(
        "secd,secf->edf", rows_in, grad_pre_gate, preferred_element_type=jnp.float32
    ).astype(jnp.bfloat16)
    grad_up = jnp.einsum(
        "secd,secf->edf", rows_in, grad_pre_up, preferred_element_type=jnp.float32
    ).astype(jnp.bfloat16)
    input_part = jnp.einsum(
        "secf,edf->secd", grad_pre_gate, w_gate, preferred_element_type=jnp.float32
    )
    input_part = input_part + jnp.einsum(
        "secf,edf->secd", grad_pre_up, w_up, preferred_element_type=jnp.float32
    )
    return (grad_gate, grad_up, grad_down, input_part)


def body_plain(
    stream_in,
    out_cot,
    route_experts,
    route_weights,
    w_gate,
    w_up,
    w_down,
    w_proj,
    conv_value,
    conv_gate,
    conv_taps,
    conv_result,
    channel_norm_gain,
):
    sp_count = lax.axis_size("sp")
    tp_count = lax.axis_size("tp")
    local_experts = w_gate.shape[0]
    experts_all = local_experts * sp_count
    token_rows, model_width = stream_in.shape
    top_count = route_experts.shape[1]
    capacity = 2 * top_count * token_rows // experts_all
    slot_of, source_of = slot_tables(route_experts, experts_all, capacity)
    occupied = source_of >= 0
    source_safe = jnp.maximum(source_of, 0)
    token_of = source_safe // top_count
    slot_weight = jnp.where(occupied, route_weights.reshape(-1)[source_safe], 0.0)
    row_buffer = jnp.where(occupied[:, None], stream_in[token_of], jnp.zeros((), jnp.bfloat16))
    cot_buffer = (slot_weight[:, None] * out_cot[token_of].astype(jnp.float32)).astype(jnp.bfloat16)
    row_buffer = row_buffer.reshape(experts_all, capacity, model_width)
    cot_buffer = cot_buffer.reshape(experts_all, capacity, model_width)
    slice_width = model_width // tp_count
    slice_start = lax.axis_index("tp") * slice_width
    row_slice = lax.dynamic_slice_in_dim(row_buffer, slice_start, slice_width, 2)
    cot_slice = lax.dynamic_slice_in_dim(cot_buffer, slice_start, slice_width, 2)
    row_slice, cot_slice = (
        lax.all_to_all(row_slice, "sp", split_axis=0, concat_axis=0, tiled=True),
        lax.all_to_all(cot_slice, "sp", split_axis=0, concat_axis=0, tiled=True),
    )
    rows_in, cot_in = (
        lax.all_gather(row_slice, "tp", axis=2, tiled=True),
        lax.all_gather(cot_slice, "tp", axis=2, tiled=True),
    )
    rows_in = rows_in.reshape(sp_count, local_experts, capacity, model_width)
    cot_in = cot_in.reshape(sp_count, local_experts, capacity, model_width)
    grad_gate, grad_up, grad_down, input_part = expert_terms_plain(rows_in, cot_in, w_gate, w_up, w_down)
    shared = lax.psum_scatter(
        input_part.astype(jnp.bfloat16), "tp", scatter_dimension=3, tiled=True
    )
    returned = shared.reshape(experts_all, capacity, slice_width)
    returned = lax.all_to_all(returned, "sp", split_axis=0, concat_axis=0, tiled=True)
    cot_cols = lax.dynamic_slice_in_dim(out_cot, slice_start, slice_width, 1)
    stream_part = combine_routes(returned, slot_of, cot_cols, token_rows, top_count)
    grad_stream = lax.all_gather(stream_part, "tp", axis=1, tiled=True)
    channel_total = conv_result.shape[0] * tp_count
    positions = conv_result.shape[1]
    conv_float = conv_result.astype(jnp.float32)
    chan_sum, chan_sq = lax.psum(
        (jnp.sum(conv_float, axis=0), jnp.sum(conv_float * conv_float, axis=0)), "tp"
    )
    chan_mean = chan_sum / channel_total
    chan_var = chan_sq / channel_total - chan_mean * chan_mean
    inverse_deviation = lax.rsqrt(chan_var + norm_eps)
    mean_removed = (conv_float - chan_mean) * inverse_deviation
    normalized_rows = mean_removed * channel_norm_gain[:, None]
    sigmoid_of_norm = jax.nn.sigmoid(normalized_rows)
    hidden = (normalized_rows * sigmoid_of_norm).astype(jnp.bfloat16)
    grad_proj = lax.psum_scatter(
        lax.dot_general(
            grad_stream, hidden, (((0,), (1,)), ((), ())), preferred_element_type=jnp.float32
        ),
        "sp",
        scatter_dimension=0,
        tiled=True,
    )
    hidden_gradient = lax.dot_general(
        w_proj, grad_stream, (((0,), (1,)), ((), ())), preferred_element_type=jnp.float32
    )
    normed_input_gradient = (
        hidden_gradient
        * sigmoid_of_norm
        * (1.0 + normalized_rows * (1.0 - sigmoid_of_norm))
        * channel_norm_gain[:, None]
    )
    average_products, cross_products = lax.psum(
        (
            jnp.sum(normed_input_gradient, axis=0),
            jnp.sum(normed_input_gradient * mean_removed, axis=0),
        ),
        "tp",
    )
    conv_output_gradient = inverse_deviation * (
        normed_input_gradient
        - average_products / channel_total
        - mean_removed * (cross_products / channel_total)
    )
    taps_count = conv_taps.shape[0]
    next_rim = from_behind(conv_output_gradient[:, : taps_count - 1], "sp", -1)
    extended = jnp.concatenate([conv_output_gradient, next_rim], axis=1)
    grad_gated = jnp.zeros_like(conv_output_gradient)
    for tap_index in range(taps_count):
        grad_gated = (
            grad_gated
            + conv_taps[tap_index][:, None] * extended[:, tap_index : tap_index + positions]
        )
    gate_sig = jax.nn.sigmoid(conv_gate.astype(jnp.float32))
    grad_value = (grad_gated * gate_sig).astype(jnp.bfloat16)
    grad_gate_in = (
        grad_gated * conv_value.astype(jnp.float32) * gate_sig * (1.0 - gate_sig)
    ).astype(jnp.bfloat16)
    return (grad_gate, grad_up, grad_down, grad_stream, grad_proj, grad_value, grad_gate_in)


def solution(mesh):
    return jax.shard_map(
        body if (mesh.shape["sp"], mesh.shape["tp"]) == (8, 4) else body_plain,
        mesh=mesh,
        in_specs=(
            P("sp", None),
            P("sp", None),
            P("sp", None),
            P("sp", None),
            P("sp", None, "tp"),
            P("sp", None, "tp"),
            P("sp", "tp", None),
            P(None, "tp"),
            P("tp", "sp"),
            P("tp", "sp"),
            P(None, "tp"),
            P("tp", "sp"),
            P("tp"),
        ),
        out_specs=(
            P("sp", None, "tp"),
            P("sp", None, "tp"),
            P("sp", "tp", None),
            P("sp", None),
            P("sp", "tp"),
            P("tp", "sp"),
            P("tp", "sp"),
        ),
        check_vma=False,
    )
```

time: 107 us -> 92.5 us (0.86)
  matrix products: 16.6 us -> 0 us
  local copies, waits for them, and re-layouts: 4.28 us -> 11.8 us
  Pallas kernels: 84.9 us -> 79.3 us
    dot_general x8 -> x0, matrix products: 16.6 us -> none  [dot(): lax.dot_general(a, b, (((ca,), (cb,)), ((), ())), preferred_element_type=...]
    pallas_call x2 -> x1, Pallas kernels: 84 us -> 76.3 us  [fused(): pl.pallas_call(functools.partial(fused_kernel, n, cap, channels * tp_coun...]
    unnamed x28 -> x24, local copies, waits for them, and re-layouts: 4.28 us -> 11.8 us
    pallas_call x1, Pallas kernels: 0.95 us -> 2.95 us  [flush(): pl.pallas_call(flush_kernel, out_shape=tuple((jax.ShapeDtypeStruct(a.shap...]
where the time goes in v1:
time: 92.5 us; the launch traced here: 91.9 us
  Pallas kernels  79.3 us (86%)
  local copies, waits for them, and re-layouts  11.8 us (13%)
    pallas_call x1, Pallas kernels, fused(): pl.pallas_call(functools.partial(fused_kernel, n, cap, channels * tp_coun...  76.3 us
    unnamed x24, local copies, waits for them, and re-layouts  11.8 us
    pallas_call x1, Pallas kernels, flush(): pl.pallas_call(flush_kernel, out_shape=tuple((jax.ShapeDtypeStruct(a.shap...  2.95 us

profile of v1, /device:TPU:0, one launch (start us, length us, event | category | flops | bytes accessed | tf_op | source)
XLA Modules:
  0.0 91.9 jit_solution(13637200063627431554)
XLA Ops:
  0.6 0.0 copy-start.2
  0.6 1.2 %copy-done.2 = bf16[2048,256]{1,0:T(8,128)(2,1)S(1)} copy-done((bf16[2048,256]{1,0:T(8,128)(2,1)S(1)}, bf16[2048,256]{1,0:T(8,128)(2,1)}, u32[]{:S(2)}) %copy-start.2) | copy-done | bytes 1048600
  1.9 0.0 copy-start.3
  1.9 1.0 %copy-done.3 = bf16[128,2048]{1,0:T(8,128)(2,1)S(1)} copy-done((bf16[128,2048]{1,0:T(8,128)(2,1)S(1)}, bf16[128,2048]{1,0:T(8,128)(2,1)}, u32[]{:S(2)}) %copy-start.3) | copy-done | bytes 524312
  2.9 0.0 copy-start.4
  2.9 1.0 %copy-done.4 = bf16[128,2048]{1,0:T(8,128)(2,1)S(1)} copy-done((bf16[128,2048]{1,0:T(8,128)(2,1)S(1)}, bf16[128,2048]{1,0:T(8,128)(2,1)}, u32[]{:S(2)}) %copy-start.4) | copy-done | bytes 524312
  3.9 0.0 copy-start.5
  4.0 0.8 copy-done.5
  4.8 0.0 copy-start.6
  4.8 0.8 copy-done.6
  5.6 0.0 copy-start.7
  5.6 0.8 copy-done.7
  6.5 0.0 copy-start.8
  6.5 0.8 copy-done.8
  7.2 0.0 copy-start.9
  7.2 0.7 copy-done.9
  7.9 0.0 copy-start.10
  7.9 0.7 copy-done.10
  8.6 0.0 copy-start.11
  8.6 0.7 copy-done.11
  9.3 76.3 %fused.1 = (bf16[2048,512]{1,0:T(8,128)(2,1)S(1)}, bf16[2048,512]{1,0:T(8,128)(2,1)}, bf16[512,2048]{1,0:T(8,128)(2,1)}, bf16[128,2048]{1,0:T(8,128)(2,1)S(1)}, ...) custom-call(s32[2,128]{1,0:T(2,128)S(1)} %bitcast.9, f32[2,128]{1,0:T(2,128)S(1)} %bitcast.10, ...), custom_call_target="tpu_custom_call" | custom-call | tf_op jit(solution)/shard_map/fused/pallas_call | solution.py:585
  85.6 0.0 copy-start
  85.6 1.6 %copy-done = bf16[2048,512]{1,0:T(8,128)(2,1)S(1)} copy-done((bf16[2048,512]{1,0:T(8,128)(2,1)S(1)}, bf16[2048,512]{1,0:T(8,128)(2,1)}, u32[]{:S(2)}) %copy-start) | copy-done | bytes 2097176
  87.2 0.0 copy-start.1
  87.2 1.6 %copy-done.1 = bf16[512,2048]{1,0:T(8,128)(2,1)S(1)} copy-done((bf16[512,2048]{1,0:T(8,128)(2,1)S(1)}, bf16[512,2048]{1,0:T(8,128)(2,1)}, u32[]{:S(2)}) %copy-start.1) | copy-done | bytes 2097176
  88.8 3.0 %flush.1 = (bf16[2048,512]{1,0:T(8,128)(2,1)}, bf16[2048,512]{1,0:T(8,128)(2,1)}, bf16[512,2048]{1,0:T(8,128)(2,1)}, bf16[128,2048]{1,0:T(8,128)(2,1)}, f32[256,...) custom-call(bf16[2048,512]{1,0:T(8,128)(2,1)S(1)} %get-tuple-element.21.refs_0_, ...), custom_call_target="tpu_custom_call" | custom-call | tf_op jit(solution)/shard_map/flush/pallas_call | solution.py:610
Async XLA Ops:
  0.6 1.2 %copy-start.2 = (bf16[2048,256]{1,0:T(8,128)(2,1)S(1)}, bf16[2048,256]{1,0:T(8,128)(2,1)}, u32[]{:S(2)}) copy-start(bf16[2048,256]{1,0:T(8,128)(2,1)} %refs_9_.1) | copy-start | bytes 3145732
  1.9 1.0 %copy-start.3 = (bf16[128,2048]{1,0:T(8,128)(2,1)S(1)}, bf16[128,2048]{1,0:T(8,128)(2,1)}, u32[]{:S(2)}) copy-start(bf16[128,2048]{1,0:T(8,128)(2,1)} %refs_2_.1) | copy-start | bytes 1572868
  2.9 1.0 %copy-start.4 = (bf16[128,2048]{1,0:T(8,128)(2,1)S(1)}, bf16[128,2048]{1,0:T(8,128)(2,1)}, u32[]{:S(2)}) copy-start(bf16[128,2048]{1,0:T(8,128)(2,1)} %refs_3_.1) | copy-start | bytes 1572868
  3.9 0.8 copy-start.5
  4.8 0.8 copy-start.6
  5.6 0.8 copy-start.7
  6.5 0.8 copy-start.8
  7.2 0.7 copy-start.9
  7.9 0.7 copy-start.10
  8.6 0.7 copy-start.11
  85.6 1.6 %copy-start = (bf16[2048,512]{1,0:T(8,128)(2,1)S(1)}, bf16[2048,512]{1,0:T(8,128)(2,1)}, u32[]{:S(2)}) copy-start(bf16[2048,512]{1,0:T(8,128)(2,1)} %get-tuple-element.22.refs_1_) | copy-start | bytes 6291460
  87.2 1.6 %copy-start.1 = (bf16[512,2048]{1,0:T(8,128)(2,1)S(1)}, bf16[512,2048]{1,0:T(8,128)(2,1)}, u32[]{:S(2)}) copy-start(bf16[512,2048]{1,0:T(8,128)(2,1)} %get-tuple-element.23.refs_2_) | copy-start | bytes 6291460

commit v2 on v1

--- a/solution.py
+++ b/solution.py
@@ -584,7 +584,7 @@
     names = [name + "_h" for name in input_names] + list(outs) + list(scratch)
     return pl.pallas_call(
         functools.partial(fused_kernel, n, cap, channels * tp_count, tuple(names)),
-        out_shape=tuple(jax.ShapeDtypeStruct(*o) for o in outs.values()),
+        out_shape=tuple(V(*o) for o in outs.values()),
         in_specs=[pl.BlockSpec(memory_space=pltpu.HBM)] * len(input_names),
         out_specs=[pl.BlockSpec(memory_space=V)] * len(outs),
         scratch_shapes=list(scratch.values()),
@@ -592,7 +592,7 @@
             collective_id=0, has_side_effects=True, vmem_limit_bytes=48 << 20
         ),
         name="fused",
-    )(*[given[name] for name in input_names])
+    )(*[pltpu.with_memory_space_constraint(given[name], pltpu.HBM) for name in input_names])
 
 
 def flush_kernel(*refs):

time: 92.5 us -> 78.8 us (0.85)
  local copies, waits for them, and re-layouts: 11.8 us -> 0 us
  Pallas kernels: 79.3 us -> 77.8 us
    unnamed x24 -> x0, local copies, waits for them, and re-layouts: 11.8 us -> none
    pallas_call x1, Pallas kernels: 76.3 us -> 74.8 us  [fused(): pl.pallas_call(functools.partial(fused_kernel, n, cap, channels * tp_coun...]
where the time goes in v2:
time: 78.8 us; the launch traced here: 78.6 us
  Pallas kernels  77.8 us (99%)
  between operations  0.81 us (1%)
    pallas_call x1, Pallas kernels, fused(): pl.pallas_call(functools.partial(fused_kernel, n, cap, channels * tp_coun...  74.8 us
    pallas_call x1, Pallas kernels, flush(): pl.pallas_call(flush_kernel, out_shape=tuple((jax.ShapeDtypeStruct(a.shap...  2.96 us

profile of v2, /device:TPU:0, one launch (start us, length us, event | category | flops | bytes accessed | tf_op | source)
XLA Modules:
  0.0 78.6 jit_solution(3118045484215942427)
XLA Ops:
  0.6 74.8 %fused.1 = (bf16[2048,512]{1,0:T(8,128)(2,1)S(1)}, bf16[2048,512]{1,0:T(8,128)(2,1)S(1)}, bf16[512,2048]{1,0:T(8,128)(2,1)S(1)}, bf16[128,2048]{1,0:T(8,128)(2,1...) custom-call(s32[2,128]{1,0:T(2,128)} %bitcast.12, f32[2,128]{1,0:T(2,128)} %bitcast.13, ...), custom_call_target="tpu_custom_call" | custom-call | tf_op jit(solution)/shard_map/fused/pallas_call | solution.py:585
  75.5 3.0 %flush.1 = (bf16[2048,512]{1,0:T(8,128)(2,1)}, bf16[2048,512]{1,0:T(8,128)(2,1)}, bf16[512,2048]{1,0:T(8,128)(2,1)}, bf16[128,2048]{1,0:T(8,128)(2,1)}, f32[256,...) custom-call(bf16[2048,512]{1,0:T(8,128)(2,1)S(1)} %get-tuple-element.21.refs_0_, ...), custom_call_target="tpu_custom_call" | custom-call | tf_op jit(solution)/shard_map/flush/pallas_call | solution.py:610

commit v3 on v2

--- a/solution.py
+++ b/solution.py
@@ -23,15 +23,18 @@
     return pl.ds(pl.multiple_of(start, size), size)
 
 
-def greet(n, s, q, tp_peers):
+def greet(n, s, q, tp_peers, ahead):
     barrier = pltpu.get_barrier_semaphore()
     for d in range(1, n):
         pl.semaphore_signal(
             barrier, inc=1, device_id={"sp": lax.rem(s + d, n), "tp": q}, device_id_type=MESH
         )
     for peer in tp_peers:
-        pl.semaphore_signal(barrier, inc=1, device_id={"sp": s, "tp": peer}, device_id_type=MESH)
-    pl.semaphore_wait(barrier, n - 1 + len(tp_peers))
+        for sp in (s, ahead):
+            pl.semaphore_signal(
+                barrier, inc=1, device_id={"sp": sp, "tp": peer}, device_id_type=MESH
+            )
+    pl.semaphore_wait(barrier, n - 1 + 2 * len(tp_peers))
 
 
 def remote(src, dst, send, recv, sp, tp):
@@ -99,12 +102,16 @@
         loads[name] = pltpu.make_async_copy(r[name + "_h"], r[name], r["load"].at[i])
         loads[name].start()
 
-    def start(src, dst, key, index, sp, tp, recv=None):
+    def start(src, dst, key, index, sp, tp, recv=None, keep=True):
         send, arrive = r["send_" + key], r["recv_" + key]
         copy = remote(src, dst, send.at[index], arrive.at[index if recv is None else recv], sp, tp)
         copy.start()
-        copies.append(copy)
+        if keep:
+            copies.append(copy)
         return copy
+
+    def sent(like, key, index):
+        remote(like, like, r["send_" + key].at[index], r["recv_" + key].at[index], s, q).wait_send()
 
     def start_if(cond, src, dst, key, index, sp, tp, recv):
         copy = remote(
@@ -118,10 +125,16 @@
 
     high = z // (nz // 2)
     folded = z + high * (nz - 1 - 2 * z)
-    far_order = [1 - folded, 2 + 0 * z, 3 + 0 * z]
-    source = [f + high * (nz - 1 - 2 * f) for f in far_order]
-    chunk_z = [z] + source
-    chunk_rows = [aligned(c * pair, pair) for c in chunk_z]
+    middle, at_end = folded == 1, folded == 0
+
+    def unfold(f):
+        return f + high * (nz - 1 - 2 * f)
+
+    source = [
+        unfold((1 - folded) * (j + 1) + folded * mid) for j, mid in enumerate((2, 0, 3))
+    ]
+    chunks_end = [z] + source
+    chunks_mid = source + [z]
 
     def block_rows(block):
         return aligned(block * cap, cap)
@@ -133,47 +146,43 @@
     meta[z] = jnp.concatenate(
         [routes_own.astype(f32), weights_own, jnp.zeros((8 - 2 * top, tokens), f32)], axis=0
     )
-    greet(n, s, q, peers)
-    meta_waits = [
-        start(meta.at[z], meta.at[z], "m", d - 1, 2 * lax.rem(z + d, nz) + x, q)
-        for d in range(1, nz)
-    ]
+    behind, ahead = lax.rem(s + n - 1, n), lax.rem(s + 1, n)
+    greet(n, s, q, peers, ahead)
+    for d in range(1, nz):
+        start(meta.at[z], meta.at[z], "m", d - 1, 2 * lax.rem(z + d, nz) + x, q, z)
     raw = r["raw"]
     values = (stream, cot)
     for a, name in enumerate(("stream", "cot")):
         loads[name].wait()
         src = values[a].at[:, quarter]
-        start_if(z < nz - 1, src, raw.at[a, z], "zo", (a, 0), s + 2, q, (a, z))
-        start_if(z > 0, src, raw.at[a, z], "zp", (a, 0), s - 2, q, (a, z))
-
-    def landed_raw(a, j):
+        start_if(z < nz - 1, src, raw.at[a, z], "z", (a, 0), s + 2, q, (a, z))
+        start_if(z > 0, src, raw.at[a, z], "z", (a, 1), s - 2, q, (a, z))
+
+    middle = (z > 0) & (z < nz - 1)
+
+    def onward(j):
+        return 2 * z - source[1] if j == 1 else source[1]
+
+    def relay_raw(j, a):
         dst = raw.at[a, source[j]]
-        from_below = source[j] < z
-
-        @pl.when(from_below)
-        def _():
-            landed(dst, "zo", (a, source[j]))
-
-        @pl.when(source[j] > z)
-        def _():
-            landed(dst, "zp", (a, source[j]))
-
-        start_if((source[j] < z) & (z < nz - 1), dst, dst, "zo", (a, j + 1), s + 2, q, (a, source[j]))
-        start_if((source[j] > z) & (z > 0), dst, dst, "zp", (a, j + 1), s - 2, q, (a, source[j]))
+        landed(dst, "z", (a, source[j]))
+        start(dst, dst, "z", (a, j + 2), 2 * onward(j) + x, q, (a, source[j]), keep=False)
 
     pick, slot_weight = slot_pick(routes_own, weights_own, 2 * z, pair, cap)
     ownbuf = r["ownbuf"]
     own_half, other_half = aligned(x * cap, cap), aligned((1 - x) * cap, cap)
-    for a in range(2):
+
+    def send_own(a):
         got = dot(pick, values[a][...])
         ownbuf[a] = (got * slot_weight if a else got).astype(bf16)
         for i, cols in enumerate((quarter, quarter_y)):
             start(
                 ownbuf.at[a, other_half, cols], full[a].at[block_rows(s), cols],
-                "xo", (a, i), sx, q,
+                "xo", (a, i), sx, q, keep=False,
             )
-    for a in range(2):
         full[a][block_rows(s), :] = ownbuf[a, own_half, :]
+
+    send_own(0)
     r["pick"][...] = slot_pick(routes_own, weights_own, 0, n * cap, cap)[0]
 
     def exchange_stats(buffer, first, second, which):
@@ -185,12 +194,14 @@
             for p, peer in enumerate(peers)
         ]
 
+    def totals(total):
+        wide = jnp.concatenate([total, jnp.zeros((tokens - 8, tokens), f32)], axis=0).T
+        return wide[:, 0:1], wide[:, 1:2]
+
     def summed_stats(buffer, waits):
         for w in waits:
             w.wait_recv()
-        total = (buffer[3] + buffer[0]) + (buffer[1] + buffer[2])
-        wide = jnp.concatenate([total, jnp.zeros((tokens - 8, tokens), f32)], axis=0).T
-        return wide[:, 0:1], wide[:, 1:2]
+        return totals((buffer[3] + buffer[0]) + (buffer[1] + buffer[2]))
 
     loads["conv"].wait()
     loads["gain"].wait()
@@ -201,40 +212,44 @@
         jnp.sum(conv * conv, axis=1, keepdims=True),
         0,
     )
-    for copy in meta_waits:
-        copy.wait_recv()
-    picks = []
-    for j in range(nz - 1):
+    pick_all, weight_all = r["picks"], r["slot_weights"]
+
+    def pick_for(j):
+        landed(meta.at[source[j]], "m", source[j])
         there = meta[source[j]]
-        picks.append(
-            slot_pick(there[0:top].astype(jnp.int32), there[top : 2 * top], 2 * z, pair, cap)
+        pick_j, weight_j = slot_pick(
+            there[0:top].astype(jnp.int32), there[top : 2 * top], 2 * z, pair, cap
         )
+        pick_all[j] = pick_j
+        weight_all[j] = jnp.broadcast_to(weight_j, weight_all.shape[1:])
+
     pickbuf = r["pickbuf"]
 
-    def arrive_raw(j, a):
-        landed_raw(a, j)
-        pick_j, weight_j = picks[j]
-        got = dot(pick_j, raw[a, source[j]])
-        pickbuf[a, j] = (got * weight_j if a else got).astype(bf16)
+    def take_raw(j, a):
+        got = dot(pick_all[j], raw[a, source[j]])
+        pickbuf[a, j] = (got * weight_all[j][:, 0:1] if a else got).astype(bf16)
         rows = block_rows(2 * source[j] + x)
         mine, other = pickbuf.at[a, j, own_half], pickbuf.at[a, j, other_half]
         here = full[a].at[rows, quarter]
-        start(other, here, "x", (a, j), sx, q)
-        start(mine, here, "y", (a, j, 0), s, q_y)
-        start(mine, here, "c", (a, j, 0), s, q_core)
+        start(other, here, "x", (a, j), sx, q, keep=False)
+        start(mine, here, "y", (a, j, 0), s, q_y, keep=False)
+        start(mine, here, "c", (a, j, 0), s, q_core, keep=False)
         full[a][rows, quarter] = pickbuf[a, j, own_half]
+
+    def arrive_raw(j, a):
+        landed(raw.at[a, source[j]], "z", (a, source[j]))
+        take_raw(j, a)
 
     def arrive_x(j, a):
         here = full[a].at[block_rows(2 * source[j] + 1 - x), quarter]
         landed(here, "x", (a, j))
-        start(here, here, "y", (a, j, 1), s, q_y)
-        start(here, here, "c", (a, j, 1), s, q_core)
-
-    def arrive_y(j, a):
-        for i in range(2):
-            here = full[a].at[block_rows(2 * source[j] + (x if i == 0 else 1 - x)), quarter_y]
-            landed(here, "y", (a, j, i))
-            start(here, here, "d", (a, j, i), s, q_core)
+        start(here, here, "y", (a, j, 1), s, q_y, keep=False)
+        start(here, here, "c", (a, j, 1), s, q_core, keep=False)
+
+    def arrive_y(j, a, i):
+        here = full[a].at[block_rows(2 * source[j] + (x if i == 0 else 1 - x)), quarter_y]
+        landed(here, "y", (a, j, i))
+        start(here, here, "d", (a, j, i), s, q_core, keep=False)
 
     def complete(j, a):
         for i in range(2):
@@ -246,7 +261,7 @@
         for i, cols in enumerate((quarter, quarter_y)):
             here = full[a].at[block_rows(sx), cols]
             landed(here, "xo", (a, i))
-            start(here, here, "xc", (a, i), s, q_core)
+            start(here, here, "xc", (a, i), s, q_core, keep=False)
 
     def complete_own(a):
         for i, owner in enumerate((q_core, q_far)):
@@ -255,27 +270,33 @@
     act_all, dg_all, du_all, part = r["act"], r["dg"], r["du"], r["part"]
     pre_gate_ref, pre_up_ref = r["pre_gate"], r["pre_up"]
 
+    chunks = chunks_end
+
+    def block_of(k, i):
+        if chunks[k] is z:
+            return s if i else sx
+        return 2 * chunks[k] + i
+
+    def chunk_of(k):
+        return aligned(chunks[k] * pair, pair)
+
+    def ready(k, a):
+        if chunks[k] is z:
+            complete_own(a)
+        else:
+            complete(k - 1 if chunks is chunks_end else k, a)
+
     def first_half(k):
-        rows = chunk_rows[k]
-        if k:
-            complete(k - 1, 0)
-        else:
-            complete_own(0)
-            loads["wg"].wait()
-            loads["wu"].wait()
-        rows_in = full[0][rows, :]
-        pre_gate_ref[...] = dot(rows_in, wg[...])
-        pre_up_ref[...] = dot(rows_in, wu[...])
+        ready(k, 0)
+        rows_in = full[0][chunk_of(k), :]
+        pre_gate_ref[k] = dot(rows_in, wg[...])
+        pre_up_ref[k] = dot(rows_in, wu[...])
 
     def second_half(k):
-        rows = chunk_rows[k]
-        if k:
-            complete(k - 1, 1)
-        else:
-            complete_own(1)
-            loads["wd"].wait()
+        ready(k, 1)
+        rows = chunk_of(k)
         grad_act = dot(full[1][rows, :], wd[...], 1, 1)
-        pre_gate, pre_up = pre_gate_ref[...], pre_up_ref[...]
+        pre_gate, pre_up = pre_gate_ref[k], pre_up_ref[k]
         glu_part = jnp.minimum(pre_gate, clamp_limit)
         lin_part = jnp.clip(pre_up, -clamp_limit, clamp_limit)
         sig_glu = jax.nn.sigmoid(alpha_gate * glu_part)
@@ -289,82 +310,104 @@
         ).astype(bf16)
         dg_all[rows, :] = dg
         du_all[rows, :] = du
-        part[rows, :] = (dot(dg, wg[...], 1, 1) + dot(du, wu[...], 1, 1)).astype(bf16)
-        for h, half in ((0, 1 - y), (1, y)):
+
+    def input_grad(k, h):
+        rows = chunk_of(k)
+        half = y if h else 1 - y
+        there = aligned(half * 2 * width, 2 * width)
+        part[rows, there] = (
+            dot(dg_all[rows, :], wg[there, :], 1, 1) + dot(du_all[rows, :], wu[there, :], 1, 1)
+        ).astype(bf16)
+        start(
+            part.at[rows, aligned((2 * half + 1 - core) * width, width)],
+            r["from_core"].at[h, rows], "rc", (k, h), s, q_core, keep=False,
+        )
+
+    def reduce_core(k, *parts):
+        if 1 not in parts:
+            landed(r["from_core"].at[0, chunk_of(k)], "rc", (k, 0))
+        for i in parts or (0, 1):
+            some = block_rows(block_of(k, i))
+            r["to_y"][some, :] = (
+                part[some, quarter_y].astype(f32) + r["from_core"][0, some, :].astype(f32)
+            ).astype(bf16)
             start(
-                part.at[rows, aligned((2 * half + 1 - core) * width, width)],
-                r["from_core"].at[h, rows], "rc", (k, h), s, q_core,
+                r["to_y"].at[some], r["from_y"].at[some], "ry", (k, i), s, q_y, keep=False
             )
-
-    def reduce_core(k):
-        rows = chunk_rows[k]
-        landed(r["from_core"].at[0, rows], "rc", (k, 0))
-        r["to_y"][rows, :] = (
-            part[rows, quarter_y].astype(f32) + r["from_core"][0, rows, :].astype(f32)
-        ).astype(bf16)
-        start(r["to_y"].at[rows], r["from_y"].at[rows], "ry", k, s, q_y)
-        landed(r["from_core"].at[1, rows], "rc", (k, 1))
-        r["own"][rows, :] = part[rows, quarter].astype(f32) + r["from_core"][
-            1, rows, :
-        ].astype(f32)
 
     ret = r["ret"]
     mine_slots = block_rows(s)
 
     def reduce_y(k):
-        rows = chunk_rows[k]
-        landed(r["from_y"].at[rows], "ry", k)
-        r["to_xz"][rows, :] = (
-            r["own"][rows, :] + r["from_y"][rows, :].astype(f32)
-        ).astype(bf16)
-        if k:
-            for i in range(2):
-                home = 2 * chunk_z[k] + i
-                start(r["to_xz"].at[block_rows(home)], ret.at[mine_slots], "r", (k, i), home, q, (s, 0))
-        else:
-            start(r["to_xz"].at[block_rows(sx)], ret.at[mine_slots], "r", (0, 0), sx, q, (s, 0))
-            ret[mine_slots, :] = r["to_xz"][mine_slots, :]
+        landed(r["from_core"].at[1, chunk_of(k)], "rc", (k, 1))
+        for i in range(2):
+            home = block_of(k, i)
+            some = block_rows(home)
+            landed(r["from_y"].at[some], "ry", (k, i))
+            r["to_xz"][some, :] = (
+                part[some, quarter].astype(f32)
+                + r["from_core"][1, some, :].astype(f32)
+                + r["from_y"][some, :].astype(f32)
+            ).astype(bf16)
+            if chunks[k] is z and i:
+                ret[mine_slots, :] = r["to_xz"][mine_slots, :]
+            else:
+                send_home(home)
+
+    def send_home(home):
+        start(
+            r["to_xz"].at[block_rows(home)], ret.at[mine_slots], "r", home, home, q, s, keep=False
+        )
 
     hid_all = r["hid"]
 
     def hid_rows(block):
         return aligned(block * tokens, tokens)
 
+    def send_hidden():
+        here = hid_all.at[hid_rows(s)]
+        start_if(z < nz - 1, here, here, "h", 0, s + 2, q, z)
+        start_if(z > 0, here, here, "h", 1, s - 2, q, z)
+
+    rim = r["rim_grad"].shape[0]
+
+    def send_rim():
+        for i, name in enumerate(("removed", "inverse")):
+            start(r[name].at[0:rim], r["rim_" + name], "e", i, behind, q, keep=False)
+
     def relay_hidden(j):
-        if j < 0:
-            here = hid_all.at[hid_rows(s)]
-            start_if(z < nz - 1, here, here, "ho", 0, s + 2, q, z)
-            start_if(z > 0, here, here, "hp", 0, s - 2, q, z)
-        else:
-            here = hid_all.at[hid_rows(2 * source[j] + x)]
-
-            @pl.when(source[j] < z)
-            def _():
-                landed(here, "ho", source[j])
-
-            @pl.when(source[j] > z)
-            def _():
-                landed(here, "hp", source[j])
-
-            start_if((source[j] < z) & (z < nz - 1), here, here, "ho", j + 1, s + 2, q, source[j])
-            start_if((source[j] > z) & (z > 0), here, here, "hp", j + 1, s - 2, q, source[j])
-        start(here, here, "hx", j + 1, sx, q)
-
-    def weight_grad(left, right, out, by_left):
+        here = hid_all.at[hid_rows(2 * source[j] + x)]
+        landed(here, "h", source[j])
+        start(here, here, "h", j + 2, 2 * onward(j) + x, q, source[j], keep=False)
+
+    def cross_hidden(k):
+        here = hid_all.at[hid_rows(2 * chunks_end[k] + x)]
+        start(here, here, "hx", k, sx, q, keep=False)
+
+    def arrive_hidden(j):
+        landed(hid_all.at[hid_rows(2 * source[j] + x)], "h", source[j])
+        cross_hidden(j + 1)
+
+    def weight_grad(left, right, out, by_left, part_of):
         tile = right.shape[1] if by_left else left.shape[1]
+        steps = model_width // tile // 2
 
         def step(i, carry):
-            there = aligned(i * tile, tile)
+            there = aligned((part_of * steps + i) * tile, tile)
             if by_left:
                 out[there, :] = dot(left[:, there], right[...], 0, 0).astype(bf16)
             else:
                 out[:, there] = dot(left[...], right[:, there], 0, 0).astype(bf16)
             return carry
 
-        lax.fori_loop(0, model_width // tile, step, 0)
-
-    arrive_raw(0, 0)
-    arrive_own(0)
+        lax.fori_loop(0, steps, step, 0)
+
+    def grad_of(which, part_of):
+        if which == "down":
+            weight_grad(r["act"], r["cots"], r["gdown"], False, part_of)
+        else:
+            weight_grad(r["rows"], r["dg" if which == "gate" else "du"], r["g" + which], True, part_of)
+
     chan_sum, chan_sq = summed_stats(r["stat"], stat_waits)
     chan_mean = chan_sum / channel_total
     chan_var = chan_sq / channel_total - chan_mean * chan_mean
@@ -377,57 +420,191 @@
     r["slope"][...] = sig * (1.0 + normed * (1.0 - sig)) * gain
     r["removed"][...] = mean_removed
     r["inverse"][...] = jnp.broadcast_to(inverse_deviation, r["inverse"].shape)
-    arrive_raw(0, 1)
-    arrive_own(1)
-    arrive_x(0, 0)
-    first_half(0)
-    arrive_raw(1, 0)
-    arrive_y(0, 0)
-    arrive_x(0, 1)
-    second_half(0)
-    arrive_raw(1, 1)
-    arrive_y(0, 1)
-    arrive_x(1, 0)
-    first_half(1)
-    arrive_raw(2, 0)
-    arrive_y(1, 0)
-    arrive_x(1, 1)
-    second_half(1)
-    arrive_raw(2, 1)
-    relay_hidden(-1)
-    arrive_y(1, 1)
-    arrive_x(2, 0)
-    reduce_core(0)
-    first_half(2)
-    arrive_x(2, 1)
-    arrive_y(2, 0)
-    second_half(2)
-    reduce_core(1)
-    arrive_y(2, 1)
-    first_half(3)
-    second_half(3)
-    reduce_y(0)
-    reduce_core(2)
-    reduce_core(3)
-    relay_hidden(0)
-    reduce_y(1)
-    weight_grad(r["act"], r["cots"], r["gdown"], False)
-    reduce_y(2)
-    relay_hidden(1)
-    reduce_y(3)
-    relay_hidden(2)
-    weight_grad(r["rows"], r["dg"], r["ggate"], True)
-    weight_grad(r["rows"], r["du"], r["gup"], True)
+    send_hidden()
+    for name in ("wg", "wu", "wd"):
+        loads[name].wait()
+
+    def end_sequence():
+        pick_for(0)
+        arrive_raw(0, 0)
+        send_own(1)
+        arrive_own(0)
+        pick_for(1)
+        pick_for(2)
+        arrive_raw(0, 1)
+        arrive_x(0, 0)
+        arrive_y(0, 0, 0)
+        first_half(0)
+        arrive_raw(1, 0)
+        arrive_own(1)
+        arrive_y(0, 1, 0)
+        arrive_x(0, 1)
+        arrive_y(0, 0, 1)
+        arrive_raw(1, 1)
+        second_half(0)
+        arrive_x(1, 0)
+        arrive_y(1, 0, 0)
+        input_grad(0, 0)
+        send_rim()
+        arrive_y(0, 1, 1)
+        arrive_raw(2, 0)
+        first_half(1)
+        arrive_x(1, 1)
+        arrive_y(1, 1, 0)
+        arrive_y(1, 0, 1)
+        arrive_raw(2, 1)
+        second_half(1)
+        cross_hidden(0)
+        arrive_x(2, 0)
+        arrive_y(2, 0, 0)
+        input_grad(1, 0)
+        arrive_hidden(0)
+        arrive_y(1, 1, 1)
+        arrive_x(2, 1)
+        first_half(2)
+        arrive_y(2, 0, 1)
+        arrive_y(2, 1, 0)
+        reduce_core(1)
+        second_half(2)
+        input_grad(2, 0)
+        input_grad(1, 1)
+        reduce_core(2)
+        reduce_core(0, 0)
+        first_half(3)
+        arrive_y(2, 1, 1)
+        arrive_hidden(1)
+        reduce_y(1)
+        second_half(3)
+        input_grad(3, 0)
+        input_grad(2, 1)
+        reduce_core(3)
+        reduce_core(0, 1)
+        reduce_y(2)
+        input_grad(3, 1)
+        grad_of("down", 0)
+        input_grad(0, 1)
+        grad_of("down", 1)
+        reduce_y(3)
+        reduce_y(0)
+        arrive_hidden(2)
+
+    def mid_sequence():
+        pick_for(0)
+        pick_for(1)
+        relay_raw(0, 0)
+        relay_raw(1, 0)
+        take_raw(0, 0)
+        take_raw(1, 0)
+        pick_for(2)
+        relay_raw(0, 1)
+        relay_raw(1, 1)
+        take_raw(0, 1)
+        take_raw(1, 1)
+        send_own(1)
+        arrive_own(0)
+        arrive_x(0, 0)
+        arrive_x(1, 0)
+        arrive_y(0, 0, 0)
+        relay_raw(2, 0)
+        take_raw(2, 0)
+        arrive_y(1, 0, 0)
+        arrive_x(0, 1)
+        arrive_x(1, 1)
+        arrive_y(0, 1, 0)
+        relay_raw(2, 1)
+        take_raw(2, 1)
+        send_rim()
+        arrive_y(1, 1, 0)
+        arrive_y(0, 0, 1)
+        relay_hidden(0)
+        relay_hidden(1)
+        arrive_own(1)
+        arrive_y(1, 0, 1)
+        arrive_x(2, 0)
+        first_half(0)
+        arrive_y(2, 0, 0)
+        arrive_x(2, 1)
+        first_half(1)
+        arrive_y(0, 1, 1)
+        cross_hidden(0)
+        cross_hidden(1)
+        cross_hidden(2)
+        second_half(0)
+        arrive_y(1, 1, 1)
+        arrive_y(2, 1, 0)
+        input_grad(0, 0)
+        relay_hidden(2)
+        cross_hidden(3)
+        second_half(1)
+        reduce_core(0)
+        input_grad(1, 0)
+        input_grad(0, 1)
+        arrive_y(2, 0, 1)
+        first_half(2)
+        reduce_core(1)
+        arrive_y(2, 1, 1)
+        input_grad(1, 1)
+        second_half(2)
+        input_grad(2, 0)
+        reduce_y(0)
+        input_grad(2, 1)
+        reduce_core(2)
+        first_half(3)
+        second_half(3)
+        reduce_y(1)
+        input_grad(3, 0)
+        input_grad(3, 1)
+        reduce_core(3)
+        reduce_y(2)
+        grad_of("down", 0)
+        grad_of("down", 1)
+        reduce_y(3)
+
+    chunks = chunks_end
+    pl.when(at_end)(end_sequence)
+    chunks = chunks_mid
+    pl.when(middle)(mid_sequence)
+    grad_of("gate", 0)
+    grad_of("gate", 1)
 
     for d in range(1, n):
         e = lax.rem(s + d, n)
-        landed(ret.at[block_rows(e)], "r", (e, 0))
+        landed(ret.at[block_rows(e)], "r", e)
     gs_ref = r["gs"]
     combined = dot(r["pick"][...], ret[...], 0, 0) + cot[:, quarter].astype(f32)
     gs_ref[:, quarter] = combined.astype(bf16)
     mine_cols = gs_ref.at[:, quarter]
     by_core = start(mine_cols, mine_cols, "g", 0, s, q_core)
     by_y = start(mine_cols, mine_cols, "g", 1, s, q_y)
+    col_all = r["col"]
+    holder, relay = q == z, q_y == z
+    for i in range(2):
+        target = 2 * q + i
+        start_if(
+            target != s, gs_ref.at[:, aligned(target * icols, icols)], col_all.at[hid_rows(s)],
+            "k", i, target, q, s,
+        )
+    blocks = [sx]
+    for j in range(nz - 1):
+        blocks += [2 * source[j] + x, 2 * source[j] + 1 - x]
+
+    def pass_cols(block):
+        there = col_all.at[hid_rows(block)]
+
+        @pl.when(holder)
+        def _():
+            landed(there, "k", block)
+            start(there, there, "fy", block, s, q_y, keep=False)
+            start(there, there, "fc", block, s, q_core, keep=False)
+
+    def relay_cols(block):
+        there = col_all.at[hid_rows(block)]
+
+        @pl.when(relay)
+        def _():
+            landed(there, "fy", block)
+            start(there, there, "fc", block, s, q_core, keep=False)
+
     loads["proj"].wait()
     proj = r["proj"]
 
@@ -435,62 +612,65 @@
         cols = aligned(owner * width, width)
         return dot(gs_ref[:, cols], proj[cols, :])
 
+    grad_of("up", 0)
+    grad_of("up", 1)
     grad_hidden = partial_of(q)
     by_y.wait_recv()
     y_cols = gs_ref.at[:, quarter_y]
     by_far = start(y_cols, y_cols, "g", 2, s, q_core)
     grad_hidden = grad_hidden + partial_of(q_y)
+    pass_cols(blocks[0])
+    pass_cols(blocks[1])
     by_core.wait_recv()
     grad_hidden = grad_hidden + partial_of(q_core)
+    pass_cols(blocks[2])
     by_far.wait_recv()
     grad_hidden = grad_hidden + partial_of(q_far)
-    half_rows = tokens // 2
-    part_rows = aligned(core * half_rows, half_rows)
-    land = aligned(s * tokens + core * half_rows, half_rows)
-    order = [lax.rem(s + d, n) for d in range(1, n)]
-    col_all = r["col"]
-    col_waits = [
-        start(
-            gs_ref.at[part_rows, aligned(order[j] * icols, icols)], col_all.at[land],
-            "k", j, order[j], q,
-        )
-        for j in range(n - 1)
-    ]
-    col_all[hid_rows(s), :] = gs_ref[:, aligned(s * icols, icols)]
+    norm_grad = grad_hidden * r["slope"][...]
     mean_removed = r["removed"][...]
     inverse_deviation = r["inverse"][:, 0:1]
-    norm_grad = grad_hidden * r["slope"][...]
+    norm_grad_ref = r["norm_grad"]
+    norm_grad_ref[...] = norm_grad
+    start(norm_grad_ref.at[0:rim], r["rim_grad"], "e", 2, behind, q)
     stat_waits = exchange_stats(
         r["stat2"],
         jnp.sum(norm_grad, axis=1, keepdims=True),
         jnp.sum(norm_grad * mean_removed, axis=1, keepdims=True),
         1,
     )
+    rim_stat = r["rim_stat"]
+    for p, peer in enumerate((q,) + peers):
+        start(r["stat2"].at[3], rim_stat.at[q], "t", p, behind, peer, q)
+    col_all[hid_rows(s), :] = gs_ref[:, aligned(s * icols, icols)]
+    for block in blocks[3:5]:
+        pass_cols(block)
+    for block in blocks[:2]:
+        relay_cols(block)
     avg, cross = summed_stats(r["stat2"], stat_waits)
-    conv_grad = inverse_deviation * (
-        norm_grad - avg / channel_total - mean_removed * (cross / channel_total)
-    )
     ext = r["ext"]
-    rim = ext.shape[0] - tokens
-    ext[0:tokens, :] = conv_grad
-    halo = remote(
-        ext.at[0:rim], ext.at[tokens : tokens + rim], r["send_e"].at[0], r["recv_e"].at[0],
-        lax.rem(s + n - 1, n), q,
-    )
-    halo.start()
-    forwards = []
-    for j in range(n - 1):
-        col_waits[j].wait_recv()
-        origin = lax.rem(s + n - (j + 1), n)
-        there = col_all.at[aligned(origin * tokens + core * half_rows, half_rows)]
-        forwards.append(start(there, there, "f", j, s, q_core))
+
+    def conv_grad_of(inverse, grad, removed, avg, cross):
+        return inverse * (grad - avg / channel_total - removed * (cross / channel_total))
+
+    ext[0:tokens, :] = conv_grad_of(inverse_deviation, norm_grad, mean_removed, avg, cross)
+    for block in blocks[5:]:
+        pass_cols(block)
+    for block in blocks[2:4]:
+        relay_cols(block)
+    for i, name in enumerate(("removed", "inverse", "grad")):
+        landed(r["rim_" + name], "e", i)
+    for owner in range(1 + len(peers)):
+        landed(rim_stat.at[owner], "t", owner)
+    avg, cross = totals((rim_stat[0] + rim_stat[1]) + (rim_stat[2] + rim_stat[3]))
+    edge = conv_grad_of(
+        r["rim_inverse"][:, 0:1], r["rim_grad"][...], r["rim_removed"][...], avg[0:rim],
+        cross[0:rim],
+    )
+    ext[tokens : tokens + rim, :] = jnp.where(s == n - 1, 0.0, edge)
+    relay_cols(blocks[4])
     loads["taps"].wait()
     loads["gate"].wait()
     loads["value"].wait()
-    halo.wait_recv()
-    edge = ext[tokens : tokens + rim, :]
-    halo.wait_send()
-    ext[tokens : tokens + rim, :] = jnp.where(s == n - 1, 0.0, edge)
     acc = jnp.zeros((tokens, ext.shape[1]), f32)
     for tap in range(taps_count):
         acc = acc + r["taps"][tap : tap + 1, :] * ext[tap : tap + tokens, :]
@@ -500,15 +680,59 @@
     r["ggin"][...] = (
         gated * r["value"][...].astype(f32) * gate_sig * (1.0 - gate_sig)
     ).astype(bf16)
-    for copy in forwards:
-        copy.wait_recv()
+    for block in blocks[5:]:
+        relay_cols(block)
+
+    @pl.when(jnp.logical_not(holder | relay))
+    def _():
+        for block in blocks:
+            landed(col_all.at[hid_rows(block)], "fc", block)
+
     for k in range(nz):
-        landed(hid_all.at[hid_rows(2 * chunk_z[k] + 1 - x)], "hx", k)
+        landed(hid_all.at[hid_rows(2 * chunks_end[k] + 1 - x)], "hx", k)
     r["gproj"][...] = dot(col_all[...], hid_all[...], 0, 0)
     for copy in copies:
         copy.wait_send()
+    piece, half_chunk = full[0].at[0:cap, 0:width], part.at[0:pair, 0:width]
+    raw_piece, hid_piece = raw.at[0, 0], hid_all.at[hid_rows(0)]
+    for a in range(2):
+        for i in range(2):
+            sent(piece, "xo", (a, i))
+            sent(piece, "xc", (a, i))
+        for j in range(nz - 1):
+            sent(piece, "x", (a, j))
+            for key in ("y", "c", "d"):
+                for i in range(2):
+                    sent(piece, key, (a, j, i))
+    for k in range(nz):
+        sent(hid_piece, "hx", k)
+        for i in range(2):
+            sent(half_chunk, "rc", (k, i))
+            sent(piece, "ry", (k, i))
+    for d in range(1, n):
+        sent(piece, "r", lax.rem(s + d, n))
+    for i, name in enumerate(("removed", "inverse")):
+        sent(r["rim_" + name], "e", i)
+
+    @pl.when(middle)
+    def _():
+        for j in range(nz - 1):
+            sent(hid_piece, "h", j + 2)
+            for a in range(2):
+                sent(raw_piece, "z", (a, j + 2))
+
     for cond, copy in conditional:
         pl.when(cond)(copy.wait_send)
+    block_cols = col_all.at[hid_rows(0)]
+    for block in blocks:
+
+        @pl.when(holder)
+        def _():
+            sent(block_cols, "fy", block)
+
+        @pl.when(holder | relay)
+        def _():
+            sent(block_cols, "fc", block)
 
 
 input_names = (
@@ -549,16 +773,17 @@
         ownbuf=V((2, 2 * cap, model_width), bf16),
         pickbuf=V((2, nz - 1, 2 * cap, width), bf16),
         pick=V((slots, tokens), bf16),
+        picks=V((nz - 1, 2 * cap, tokens), bf16),
+        slot_weights=V((nz - 1, 2 * cap, tokens), f32),
         rows=V((slots, model_width), bf16),
         cots=V((slots, model_width), bf16),
         act=V((slots, hidden_width), bf16),
         dg=V((slots, hidden_width), bf16),
         du=V((slots, hidden_width), bf16),
         part=V((slots, model_width), bf16),
-        pre_gate=V((2 * cap, hidden_width), f32),
-        pre_up=V((2 * cap, hidden_width), f32),
+        pre_gate=V((nz, 2 * cap, hidden_width), f32),
+        pre_up=V((nz, 2 * cap, hidden_width), f32),
         from_core=V((2, slots, width), bf16),
-        own=V((slots, width), f32),
         to_y=V((slots, width), bf16),
         from_y=V((slots, width), bf16),
         to_xz=V((slots, width), bf16),
@@ -570,13 +795,18 @@
         inverse=V((tokens, tokens), f32),
         stat=V((4, 8, tokens), f32),
         stat2=V((4, 8, tokens), f32),
+        norm_grad=V((tokens, channels), f32),
+        rim_removed=V((rim, channels), f32),
+        rim_inverse=V((rim, tokens), f32),
+        rim_grad=V((rim, channels), f32),
+        rim_stat=V((tp_count, 8, tokens), f32),
         ext=V((tokens + rim, channels), f32),
         load=dma((len(input_names),)),
     )
     sems = dict(
-        m=(nz - 1,), zo=(2, nz), zp=(2, nz), xo=(2, 2), xc=(2, 2), x=(2, nz - 1), y=(2, nz - 1, 2),
-        c=(2, nz - 1, 2), d=(2, nz - 1, 2), s=(2, 3), rc=(nz, 2), ry=(nz,), ho=(nz,), hp=(nz,),
-        hx=(nz,), g=(3,), k=(n - 1,), f=(n - 1,), e=(1,), r=(n, 2),
+        m=(nz,), z=(2, nz + 1), xo=(2, 2), xc=(2, 2), x=(2, nz - 1), y=(2, nz - 1, 2),
+        c=(2, nz - 1, 2), d=(2, nz - 1, 2), s=(2, 3), rc=(nz, 2), ry=(nz, 2), h=(nz + 1,),
+        hx=(nz,), g=(3,), k=(n,), fy=(n,), fc=(n,), e=(3,), t=(tp_count,), r=(n,),
     )
     for key, shape in sems.items():
         scratch["send_" + key] = dma(shape)

time: 78.8 us -> 71.2 us (0.904); the launches traced: 78.6 us -> 69.7 us
  Pallas kernels: 77.8 us -> 68.9 us
    pallas_call x1, Pallas kernels: 74.8 us -> 66 us  [fused(): pl.pallas_call(functools.partial(fused_kernel, n, cap, channels * tp_coun...]
where the time goes in v3:
time: 71.2 us; the launch traced here: 69.7 us
  Pallas kernels  68.9 us (97%)
  between operations  0.83 us (1%)
    pallas_call x1, Pallas kernels, fused(): pl.pallas_call(functools.partial(fused_kernel, n, cap, channels * tp_coun...  66 us
    pallas_call x1, Pallas kernels, flush(): pl.pallas_call(flush_kernel, out_shape=tuple((jax.ShapeDtypeStruct(a.shap...  2.96 us

profile of v3, /device:TPU:0, one launch (start us, length us, event | category | flops | bytes accessed | tf_op | source)
XLA Modules:
  0.0 69.7 jit_solution(8371737500439590439)
XLA Ops:
  0.6 66.0 %fused.1 = (bf16[2048,512]{1,0:T(8,128)(2,1)S(1)}, bf16[2048,512]{1,0:T(8,128)(2,1)S(1)}, bf16[512,2048]{1,0:T(8,128)(2,1)S(1)}, bf16[128,2048]{1,0:T(8,128)(2,1...) custom-call(s32[2,128]{1,0:T(2,128)} %bitcast.12, f32[2,128]{1,0:T(2,128)} %bitcast.13, ...), custom_call_target="tpu_custom_call" | custom-call | tf_op jit(solution)/shard_map/fused/pallas_call | solution.py:815
  66.6 3.0 %flush.1 = (bf16[2048,512]{1,0:T(8,128)(2,1)}, bf16[2048,512]{1,0:T(8,128)(2,1)}, bf16[512,2048]{1,0:T(8,128)(2,1)}, bf16[128,2048]{1,0:T(8,128)(2,1)}, f32[256,...) custom-call(bf16[2048,512]{1,0:T(8,128)(2,1)S(1)} %get-tuple-element.21.refs_0_, ...), custom_call_target="tpu_custom_call" | custom-call | tf_op jit(solution)/shard_map/flush/pallas_call | solution.py:840

commit v4 on v3

--- a/solution.py
+++ b/solution.py
@@ -88,9 +88,8 @@
     tokens, model_width = stream.shape
     width = r["ret"].shape[-1]
     top = r["routes"].shape[0]
-    icols = r["gproj"].shape[0]
+    icols = r["col"].shape[1]
     pair = 2 * cap
-    taps_count = r["taps"].shape[0]
     quarter, quarter_y = aligned(q * width, width), aligned(q_y * width, width)
     wg, wu, wd = r["wg"], r["wu"], r["wd"]
     full = (r["rows"], r["cots"])
@@ -469,22 +468,21 @@
         input_grad(2, 0)
         input_grad(1, 1)
         reduce_core(2)
-        reduce_core(0, 0)
+        arrive_y(2, 1, 1)
         first_half(3)
-        arrive_y(2, 1, 1)
-        arrive_hidden(1)
-        reduce_y(1)
         second_half(3)
         input_grad(3, 0)
+        reduce_y(1)
+        arrive_hidden(1)
         input_grad(2, 1)
         reduce_core(3)
-        reduce_core(0, 1)
+        reduce_core(0)
         reduce_y(2)
         input_grad(3, 1)
         grad_of("down", 0)
         input_grad(0, 1)
+        reduce_y(3)
         grad_of("down", 1)
-        reduce_y(3)
         reduce_y(0)
         arrive_hidden(2)
 
@@ -518,39 +516,39 @@
         arrive_y(0, 0, 1)
         relay_hidden(0)
         relay_hidden(1)
+        arrive_x(2, 0)
+        arrive_y(1, 0, 1)
         arrive_own(1)
-        arrive_y(1, 0, 1)
-        arrive_x(2, 0)
-        first_half(0)
         arrive_y(2, 0, 0)
         arrive_x(2, 1)
+        first_half(0)
         first_half(1)
         arrive_y(0, 1, 1)
         cross_hidden(0)
         cross_hidden(1)
         cross_hidden(2)
+        first_half(3)
+        arrive_y(1, 1, 1)
         second_half(0)
-        arrive_y(1, 1, 1)
+        input_grad(0, 0)
         arrive_y(2, 1, 0)
-        input_grad(0, 0)
         relay_hidden(2)
         cross_hidden(3)
         second_half(1)
+        input_grad(1, 0)
         reduce_core(0)
-        input_grad(1, 0)
         input_grad(0, 1)
         arrive_y(2, 0, 1)
+        reduce_core(1)
         first_half(2)
-        reduce_core(1)
         arrive_y(2, 1, 1)
         input_grad(1, 1)
         second_half(2)
         input_grad(2, 0)
         reduce_y(0)
+        second_half(3)
+        reduce_core(2)
         input_grad(2, 1)
-        reduce_core(2)
-        first_half(3)
-        second_half(3)
         reduce_y(1)
         input_grad(3, 0)
         input_grad(3, 1)
@@ -588,19 +586,19 @@
     for j in range(nz - 1):
         blocks += [2 * source[j] + x, 2 * source[j] + 1 - x]
 
-    def pass_cols(block):
+    def pass_cols(block, where):
         there = col_all.at[hid_rows(block)]
 
-        @pl.when(holder)
+        @pl.when(holder & where)
         def _():
             landed(there, "k", block)
             start(there, there, "fy", block, s, q_y, keep=False)
             start(there, there, "fc", block, s, q_core, keep=False)
 
-    def relay_cols(block):
+    def relay_cols(block, where):
         there = col_all.at[hid_rows(block)]
 
-        @pl.when(relay)
+        @pl.when(relay & where)
         def _():
             landed(there, "fy", block)
             start(there, there, "fc", block, s, q_core, keep=False)
@@ -614,16 +612,16 @@
 
     grad_of("up", 0)
     grad_of("up", 1)
+    for block in blocks[1:5]:
+        pass_cols(block, at_end)
     grad_hidden = partial_of(q)
     by_y.wait_recv()
     y_cols = gs_ref.at[:, quarter_y]
     by_far = start(y_cols, y_cols, "g", 2, s, q_core)
     grad_hidden = grad_hidden + partial_of(q_y)
-    pass_cols(blocks[0])
-    pass_cols(blocks[1])
     by_core.wait_recv()
     grad_hidden = grad_hidden + partial_of(q_core)
-    pass_cols(blocks[2])
+    pass_cols(blocks[0], holder)
     by_far.wait_recv()
     grad_hidden = grad_hidden + partial_of(q_far)
     norm_grad = grad_hidden * r["slope"][...]
@@ -642,10 +640,15 @@
     for p, peer in enumerate((q,) + peers):
         start(r["stat2"].at[3], rim_stat.at[q], "t", p, behind, peer, q)
     col_all[hid_rows(s), :] = gs_ref[:, aligned(s * icols, icols)]
-    for block in blocks[3:5]:
-        pass_cols(block)
-    for block in blocks[:2]:
-        relay_cols(block)
+    late_first = blocks[3:5] + blocks[1:3] + blocks[5:]
+    for block in late_first:
+        pass_cols(block, middle)
+    for block in blocks[5:]:
+        pass_cols(block, at_end)
+    for block in blocks[1:5] + blocks[:1] + blocks[5:]:
+        relay_cols(block, at_end)
+    for block in blocks[:1] + late_first:
+        relay_cols(block, middle)
     avg, cross = summed_stats(r["stat2"], stat_waits)
     ext = r["ext"]
 
@@ -653,10 +656,6 @@
         return inverse * (grad - avg / channel_total - removed * (cross / channel_total))
 
     ext[0:tokens, :] = conv_grad_of(inverse_deviation, norm_grad, mean_removed, avg, cross)
-    for block in blocks[5:]:
-        pass_cols(block)
-    for block in blocks[2:4]:
-        relay_cols(block)
     for i, name in enumerate(("removed", "inverse", "grad")):
         landed(r["rim_" + name], "e", i)
     for owner in range(1 + len(peers)):
@@ -667,21 +666,8 @@
         cross[0:rim],
     )
     ext[tokens : tokens + rim, :] = jnp.where(s == n - 1, 0.0, edge)
-    relay_cols(blocks[4])
-    loads["taps"].wait()
-    loads["gate"].wait()
-    loads["value"].wait()
-    acc = jnp.zeros((tokens, ext.shape[1]), f32)
-    for tap in range(taps_count):
-        acc = acc + r["taps"][tap : tap + 1, :] * ext[tap : tap + tokens, :]
-    gated = acc.T
-    gate_sig = jax.nn.sigmoid(r["gate"][...].astype(f32))
-    r["gvalue"][...] = (gated * gate_sig).astype(bf16)
-    r["ggin"][...] = (
-        gated * r["value"][...].astype(f32) * gate_sig * (1.0 - gate_sig)
-    ).astype(bf16)
-    for block in blocks[5:]:
-        relay_cols(block)
+    for name in ("taps", "gate", "value"):
+        loads[name].wait()
 
     @pl.when(jnp.logical_not(holder | relay))
     def _():
@@ -690,7 +676,6 @@
 
     for k in range(nz):
         landed(hid_all.at[hid_rows(2 * chunks_end[k] + 1 - x)], "hx", k)
-    r["gproj"][...] = dot(col_all[...], hid_all[...], 0, 0)
     for copy in copies:
         copy.wait_send()
     piece, half_chunk = full[0].at[0:cap, 0:width], part.at[0:pair, 0:width]
@@ -762,11 +747,16 @@
         gup=((model_width, hidden_width), bf16),
         gdown=((hidden_width, model_width), bf16),
         gs=((tokens, model_width), bf16),
-        gproj=((icols, channels), f32),
-        gvalue=((channels, tokens), bf16),
-        ggin=((channels, tokens), bf16),
-    )
-    scratch = {name: V(given[name].shape, given[name].dtype) for name in input_names}
+        col=((n * tokens, icols), bf16),
+        hid=((n * tokens, channels), bf16),
+        ext=((tokens + rim, channels), f32),
+        taps=(taps.shape, taps.dtype),
+        gate=(gate.shape, gate.dtype),
+        value=(value.shape, value.dtype),
+    )
+    scratch = {
+        name: V(given[name].shape, given[name].dtype) for name in input_names if name not in outs
+    }
     scratch.update(
         meta=V((nz, 8, tokens), f32),
         raw=V((2, nz, tokens, width), bf16),
@@ -788,8 +778,6 @@
         from_y=V((slots, width), bf16),
         to_xz=V((slots, width), bf16),
         ret=V((slots, width), bf16),
-        hid=V((n * tokens, channels), bf16),
-        col=V((n * tokens, icols), bf16),
         slope=V((tokens, channels), f32),
         removed=V((tokens, channels), f32),
         inverse=V((tokens, tokens), f32),
@@ -800,7 +788,6 @@
         rim_inverse=V((rim, tokens), f32),
         rim_grad=V((rim, channels), f32),
         rim_stat=V((tp_count, 8, tokens), f32),
-        ext=V((tokens + rim, channels), f32),
         load=dma((len(input_names),)),
     )
     sems = dict(
@@ -825,26 +812,50 @@
     )(*[pltpu.with_memory_space_constraint(given[name], pltpu.HBM) for name in input_names])
 
 
-def flush_kernel(*refs):
-    count = len(refs) // 2
-    copies = [
-        pltpu.make_async_copy(refs[i], refs[count + i], refs[-1].at[i]) for i in range(count)
-    ]
-    for copy in copies:
-        copy.start()
+def finish_kernel(count, *refs):
+    given, outs, scratch = refs[: count + 6], refs[count + 6 : 2 * count + 9], refs[2 * count + 9 :]
+    col_ref, hid_ref, ext_ref, taps_ref, gate_ref, value_ref = given[count:]
+    gproj_ref, gvalue_ref, ggin_ref, sem = scratch
+    copies = []
+
+    def put(src, i):
+        copies.append(pltpu.make_async_copy(src, outs[i], sem.at[i]))
+        copies[-1].start()
+
+    for i in range(count):
+        put(given[i], i)
+    gproj_ref[...] = dot(col_ref[...], hid_ref[...], 0, 0)
+    put(gproj_ref, count)
+    tokens = gate_ref.shape[1]
+    acc = jnp.zeros((tokens, ext_ref.shape[1]), f32)
+    for tap in range(taps_ref.shape[0]):
+        acc = acc + taps_ref[tap : tap + 1, :] * ext_ref[tap : tap + tokens, :]
+    gated = acc.T
+    gate_sig = jax.nn.sigmoid(gate_ref[...].astype(f32))
+    gvalue_ref[...] = (gated * gate_sig).astype(bf16)
+    put(gvalue_ref, count + 1)
+    ggin_ref[...] = (
+        gated * value_ref[...].astype(f32) * gate_sig * (1.0 - gate_sig)
+    ).astype(bf16)
+    put(ggin_ref, count + 2)
     for copy in copies:
         copy.wait()
 
 
-def flush(*arrays):
+def finish(*arrays):
+    count = len(arrays) - 6
+    col, hid, value = arrays[count], arrays[count + 1], arrays[-1]
+    made = [((col.shape[1], hid.shape[1]), f32), (value.shape, bf16), (value.shape, bf16)]
     return pl.pallas_call(
-        flush_kernel,
-        out_shape=tuple(jax.ShapeDtypeStruct(a.shape, a.dtype) for a in arrays),
+        functools.partial(finish_kernel, count),
+        out_shape=tuple(jax.ShapeDtypeStruct(a.shape, a.dtype) for a in arrays[:count])
+        + tuple(jax.ShapeDtypeStruct(*m) for m in made),
         in_specs=[pl.BlockSpec(memory_space=pltpu.VMEM)] * len(arrays),
-        out_specs=[pl.BlockSpec(memory_space=pltpu.HBM)] * len(arrays),
-        scratch_shapes=[pltpu.SemaphoreType.DMA((len(arrays),))],
-        compiler_params=pltpu.CompilerParams(vmem_limit_bytes=4 << 20),
-        name="flush",
+        out_specs=[pl.BlockSpec(memory_space=pltpu.HBM)] * (count + 3),
+        scratch_shapes=[pltpu.VMEM(*m) for m in made]
+        + [pltpu.SemaphoreType.DMA((count + 3,))],
+        compiler_params=pltpu.CompilerParams(vmem_limit_bytes=6 << 20),
+        name="finish",
     )(*arrays)
 
 
@@ -857,7 +868,7 @@
     experts = w_gate.shape[0] * n
     tokens, model_width = stream_in.shape
     cap = 2 * route_experts.shape[1] * tokens // experts
-    outs = flush(
+    outs = finish(
         *fused(
             route_experts.T, route_weights.T, stream_in, out_cot, w_gate[0], w_up[0], w_down[0],
             w_proj, conv_value, conv_gate, conv_taps, conv_result, channel_norm_gain[None, :],

time: 71.2 us -> 68.7 us (0.965)
  Pallas kernels: 68.9 us -> 67.1 us
    pallas_call x1, Pallas kernels: 66 us -> 64.2 us  [fused(): pl.pallas_call(functools.partial(fused_kernel, n, cap, channels * tp_coun...]
where the time goes in v4:
time: 68.7 us; the launch traced here: 67.9 us
  Pallas kernels  67.1 us (98%)
  between operations  0.81 us (1%)
    pallas_call x1, Pallas kernels, fused(): pl.pallas_call(functools.partial(fused_kernel, n, cap, channels * tp_coun...  64.2 us
    pallas_call x1, Pallas kernels, finish(): pl.pallas_call(functools.partial(finish_kernel, count), out_shape=tuple((...  2.98 us

profile of v4, /device:TPU:0, one launch (start us, length us, event | category | flops | bytes accessed | tf_op | source)
XLA Modules:
  0.0 67.9 jit_solution(3304147768846071408)
XLA Ops:
  0.6 64.2 %fused.1 = (bf16[2048,512]{1,0:T(8,128)(2,1)S(1)}, bf16[2048,512]{1,0:T(8,128)(2,1)S(1)}, bf16[512,2048]{1,0:T(8,128)(2,1)S(1)}, bf16[128,2048]{1,0:T(8,128)(2,1...) custom-call(s32[2,128]{1,0:T(2,128)} %bitcast.12, ...), custom_call_target="tpu_custom_call" | custom-call | tf_op jit(solution)/shard_map/fused/pallas_call | solution.py:802
  64.8 3.0 %finish.1 = (bf16[2048,512]{1,0:T(8,128)(2,1)}, bf16[2048,512]{1,0:T(8,128)(2,1)}, bf16[512,2048]{1,0:T(8,128)(2,1)}, bf16[128,2048]{1,0:T(8,128)(2,1)}, f32[256...) custom-call(bf16[2048,512]{1,0:T(8,128)(2,1)S(1)} %get-tuple-element.24.refs_0_, ...), custom_call_target="tpu_custom_call" | custom-call | tf_op jit(solution)/shard_map/finish/pallas_call | solution.py:849

commit v5 on v4

--- a/solution.py
+++ b/solution.py
@@ -586,14 +586,24 @@
     for j in range(nz - 1):
         blocks += [2 * source[j] + x, 2 * source[j] + 1 - x]
 
-    def pass_cols(block, where):
-        there = col_all.at[hid_rows(block)]
+    def crosses(i):
+        return at_end if 3 <= i < 5 else i >= 5
+
+    def pass_cols(i, where):
+        there = col_all.at[hid_rows(blocks[i])]
 
         @pl.when(holder & where)
         def _():
-            landed(there, "k", block)
-            start(there, there, "fy", block, s, q_y, keep=False)
-            start(there, there, "fc", block, s, q_core, keep=False)
+            landed(there, "k", blocks[i])
+            if crosses(i) is not False:
+                copy = remote(
+                    there, there, r["send_fy"].at[blocks[i]], r["recv_fy"].at[blocks[i]], s, q_y
+                )
+                if crosses(i) is True:
+                    copy.start()
+                else:
+                    pl.when(crosses(i))(copy.start)
+            start(there, there, "fc", blocks[i], s, q_core, keep=False)
 
     def relay_cols(block, where):
         there = col_all.at[hid_rows(block)]
@@ -612,16 +622,26 @@
 
     grad_of("up", 0)
     grad_of("up", 1)
-    for block in blocks[1:5]:
-        pass_cols(block, at_end)
+    for i in range(1, 5):
+        pass_cols(i, at_end)
     grad_hidden = partial_of(q)
     by_y.wait_recv()
+    near = (z - q_y) * (z - q_y) <= 1
+    for i in range(2):
+        target = 2 * q_y + i
+        copy = remote(
+            gs_ref.at[:, aligned(target * icols, icols)], col_all.at[hid_rows(s)],
+            r["send_near"].at[i], r["recv_fy"].at[s], target, q,
+        )
+        go = near & (target != s)
+        pl.when(go)(copy.start)
+        conditional.append((go, copy))
     y_cols = gs_ref.at[:, quarter_y]
     by_far = start(y_cols, y_cols, "g", 2, s, q_core)
     grad_hidden = grad_hidden + partial_of(q_y)
     by_core.wait_recv()
     grad_hidden = grad_hidden + partial_of(q_core)
-    pass_cols(blocks[0], holder)
+    pass_cols(0, holder)
     by_far.wait_recv()
     grad_hidden = grad_hidden + partial_of(q_far)
     norm_grad = grad_hidden * r["slope"][...]
@@ -640,15 +660,14 @@
     for p, peer in enumerate((q,) + peers):
         start(r["stat2"].at[3], rim_stat.at[q], "t", p, behind, peer, q)
     col_all[hid_rows(s), :] = gs_ref[:, aligned(s * icols, icols)]
-    late_first = blocks[3:5] + blocks[1:3] + blocks[5:]
-    for block in late_first:
-        pass_cols(block, middle)
-    for block in blocks[5:]:
-        pass_cols(block, at_end)
-    for block in blocks[1:5] + blocks[:1] + blocks[5:]:
-        relay_cols(block, at_end)
-    for block in blocks[:1] + late_first:
-        relay_cols(block, middle)
+    for i in (3, 4, 1, 2, 5, 6):
+        pass_cols(i, middle)
+    for i in (5, 6):
+        pass_cols(i, at_end)
+    for i in (3, 4, 5, 6, 0, 1, 2):
+        relay_cols(blocks[i], at_end)
+    for i in (0, 1, 2, 5, 6, 3, 4):
+        relay_cols(blocks[i], middle)
     avg, cross = summed_stats(r["stat2"], stat_waits)
     ext = r["ext"]
 
@@ -709,11 +728,12 @@
     for cond, copy in conditional:
         pl.when(cond)(copy.wait_send)
     block_cols = col_all.at[hid_rows(0)]
-    for block in blocks:
-
-        @pl.when(holder)
-        def _():
-            sent(block_cols, "fy", block)
+    for i, block in enumerate(blocks):
+        if crosses(i) is not False:
+
+            @pl.when(holder & crosses(i))
+            def _():
+                sent(block_cols, "fy", block)
 
         @pl.when(holder | relay)
         def _():
@@ -789,6 +809,7 @@
         rim_grad=V((rim, channels), f32),
         rim_stat=V((tp_count, 8, tokens), f32),
         load=dma((len(input_names),)),
+        send_near=dma((2,)),
     )
     sems = dict(
         m=(nz,), z=(2, nz + 1), xo=(2, 2), xc=(2, 2), x=(2, nz - 1), y=(2, nz - 1, 2),

time: 68.7 us -> 68.3 us (level)
  no operation moved by 1% of the time
where the time goes in v5:
time: 68.3 us; the launch traced here: 68 us
  Pallas kernels  67.2 us (98%)
  between operations  0.81 us (1%)
    pallas_call x1, Pallas kernels, fused(): pl.pallas_call(functools.partial(fused_kernel, n, cap, channels * tp_coun...  64.3 us
    pallas_call x1, Pallas kernels, finish(): pl.pallas_call(functools.partial(finish_kernel, count), out_shape=tuple((...  2.98 us

profile of v5, /device:TPU:0, one launch (start us, length us, event | category | flops | bytes accessed | tf_op | source)
XLA Modules:
  0.0 68.0 jit_solution(2216416705052434128)
XLA Ops:
  0.6 64.3 %fused.1 = (bf16[2048,512]{1,0:T(8,128)(2,1)S(1)}, bf16[2048,512]{1,0:T(8,128)(2,1)S(1)}, bf16[512,2048]{1,0:T(8,128)(2,1)S(1)}, bf16[128,2048]{1,0:T(8,128)(2,1...) custom-call(s32[2,128]{1,0:T(2,128)} %bitcast.12, ...), custom_call_target="tpu_custom_call" | custom-call | tf_op jit(solution)/shard_map/fused/pallas_call | solution.py:823
  64.9 3.0 %finish.1 = (bf16[2048,512]{1,0:T(8,128)(2,1)}, bf16[2048,512]{1,0:T(8,128)(2,1)}, bf16[512,2048]{1,0:T(8,128)(2,1)}, bf16[128,2048]{1,0:T(8,128)(2,1)}, f32[256...) custom-call(bf16[2048,512]{1,0:T(8,128)(2,1)S(1)} %get-tuple-element.24.refs_0_, ...), custom_call_target="tpu_custom_call" | custom-call | tf_op jit(solution)/shard_map/finish/pallas_call | solution.py:870
